TPU v7x, 128 devices: a whole 4x4x4 slice. The times are simulated.
128 devices in a mesh: ep: 16 (over z, x), tp: 8 (over y, core).
Axes of the slice: x: 4, y: 4, z: 4, core: 2. Of those that a mesh axis runs over, the one named last changes fastest.
Arguments:
- glu_value: bfloat16 [131072, 1024], P(('ep', 'tp')), may hold values from -6 to 6
- glu_gate: bfloat16 [131072, 1024], P(('ep', 'tp')), may hold values from -6 to 6
- conv_taps: float32 [31, 1024], replicated, may hold values from -12 to 12
- chan_gain: float32 [1024], replicated, may hold values from 0.1 to 1.9
- chan_shift: float32 [1024], replicated, may hold values from -3 to 3
- mix_out_weight: bfloat16 [1024, 2048], P('tp'), may hold values from -0.1875 to 0.1875
- moe_input: bfloat16 [16384, 2048], P(('ep', 'tp')), may hold values from -6 to 6
- moe_gain: float32 [2048], replicated, may hold values from 0.1 to 1.9
- expert_ids: int32 [16384, 4], P(('ep', 'tp')), may hold values from 0 to 127, all different within a row; in each aligned block of 128 rows (0 to 127, 128 to 255, ...) at most 5 rows name the same one
- expert_share: float32 [16384, 4], P(('ep', 'tp')), may hold values from 0.05 to 1
- expert_gate_weight: bfloat16 [128, 2048, 1024], P(('ep', 'tp')), may hold values from -0.375 to 0.375
- expert_up_weight: bfloat16 [128, 2048, 1024], P(('ep', 'tp')), may hold values from -0.375 to 0.375
- expert_down_weight: bfloat16 [128, 1024, 2048], P(('ep', 'tp')), may hold values from -0.0390625 to 0.0390625
Outputs:
- mixed: bfloat16 [131072, 2048], P(('ep', 'tp'))
- moe_output: bfloat16 [16384, 2048], P(('ep', 'tp'))
Inputs may be any that keep to these rules, and one draw needn't show every extreme that they name: `expert_ids`: each row names 4 different experts. In each aligned block of 128 rows (the rows of one device) no expert is named by more than 5 rows, and in some block one expert is named by exactly 5 rows.
All inputs are finite; a program needn't handle non-finite values.
Results may differ from a plain program's by a relative error of at most 0.0071.
Values may be sent and summed in bfloat16 or wider, within the bound.
A program may use at most 192 MiB of HBM per device.

v0:
```python
import jax
import jax.numpy as jnp
from jax import lax
from jax.sharding import PartitionSpec as P

CLAMP_LIMIT = 7.0
GLU_SLOPE = 1.702


def passed_along(value, axis, steps):
    count = lax.axis_size(axis)
    first, last = (max(0, -steps), min(count, count - steps))
    return lax.ppermute(value, axis, [(source, source + steps) for source in range(first, last)])


def expert_apply(flat_rows, gate_matrix, up_matrix, down_matrix):
    pre_gate = jnp.dot(flat_rows, gate_matrix, preferred_element_type=jnp.float32)
    pre_up = jnp.dot(flat_rows, up_matrix, preferred_element_type=jnp.float32)
    gated = jnp.minimum(pre_gate, CLAMP_LIMIT)
    lifted = jnp.clip(pre_up, -CLAMP_LIMIT, CLAMP_LIMIT) + 1.0
    hidden = (lifted * gated * jax.nn.sigmoid(GLU_SLOPE * gated)).astype(jnp.bfloat16)
    return jnp.dot(hidden, down_matrix, preferred_element_type=jnp.float32).astype(jnp.bfloat16)


def body(
    glu_value,
    glu_gate,
    conv_taps,
    chan_gain,
    chan_shift,
    mix_out_weight,
    moe_input,
    moe_gain,
    expert_ids,
    expert_share,
    expert_gate_weight,
    expert_up_weight,
    expert_down_weight,
):
    positions = glu_value.shape[0]
    margin = conv_taps.shape[0] - 1
    borders = jnp.stack([glu_value[positions - margin :], glu_gate[positions - margin :]])
    earlier = passed_along(borders, ("ep", "tp"), 1)
    values_all = jnp.concatenate([earlier[0], glu_value], 0).astype(jnp.float32)
    gates_all = jnp.concatenate([earlier[1], glu_gate], 0).astype(jnp.float32)
    gated_input = values_all * jax.nn.sigmoid(gates_all)
    convolved = jnp.zeros(glu_value.shape, jnp.float32)
    for offset in range(margin + 1):
        convolved = convolved + conv_taps[offset] * gated_input[offset : offset + positions]
    center = jnp.mean(convolved, axis=-1, keepdims=True)
    spread = jnp.mean(jnp.square(convolved - center), axis=-1, keepdims=True)
    normalized = (convolved - center) * lax.rsqrt(spread + 1e-05) * chan_gain + chan_shift
    activated = jax.nn.silu(normalized).astype(jnp.bfloat16)
    mixed = jnp.dot(
        activated,
        lax.all_gather(mix_out_weight, "tp", axis=0, tiled=True),
        preferred_element_type=jnp.float32,
    ).astype(jnp.bfloat16)
    features = moe_input.astype(jnp.float32)
    scaled = features * lax.rsqrt(jnp.mean(jnp.square(features), axis=-1, keepdims=True) + 1e-06)
    moe_normed = (scaled * moe_gain).astype(jnp.bfloat16)
    tokens, per_token = expert_ids.shape
    model_width = moe_normed.shape[1]
    ep_size = lax.axis_size("ep")
    tp_size = lax.axis_size("tp")
    experts = ep_size * tp_size
    capacity = max(2, 5 * tokens * per_token // (4 * experts))
    copies = tokens * per_token
    flat_ids = expert_ids.reshape(copies)
    onehot = (flat_ids[:, None] == jnp.arange(experts, dtype=jnp.int32)[None, :]).astype(jnp.int32)
    earlier_count = jnp.sum((jnp.cumsum(onehot, axis=0) - onehot) * onehot, axis=1)
    slot_index = flat_ids * capacity + earlier_count
    slot_owner = (
        jnp.zeros((experts * capacity,), jnp.int32)
        .at[slot_index]
        .set(jnp.arange(copies, dtype=jnp.int32))
    )
    filled = jnp.zeros((experts * capacity,), jnp.bool_).at[slot_index].set(True)
    outgoing = jnp.where(
        filled[:, None], moe_normed[slot_owner // per_token], jnp.zeros((), jnp.bfloat16)
    )
    gate_matrix = expert_gate_weight[0]
    up_matrix = expert_up_weight[0]
    down_matrix = expert_down_weight[0]
    arrived = lax.all_to_all(
        outgoing.reshape(experts, capacity, model_width),
        ("ep", "tp"),
        split_axis=0,
        concat_axis=0,
        tiled=True,
    )
    sources = arrived.shape[0]
    held_slots = arrived.shape[1]
    answers = expert_apply(
        arrived.reshape(sources * held_slots, model_width), gate_matrix, up_matrix, down_matrix
    )
    answers = answers.reshape(sources, held_slots, model_width)
    returned = lax.all_to_all(answers, ("ep", "tp"), split_axis=0, concat_axis=0, tiled=True)
    picked = returned.reshape(experts * capacity, model_width)[slot_index].reshape(
        tokens, per_token, model_width
    )
    combined = jnp.zeros((tokens, model_width), jnp.float32)
    for choose in range(per_token):
        combined = combined + expert_share[:, choose : choose + 1] * picked[:, choose].astype(
            jnp.float32
        )
    return (mixed, combined.astype(jnp.bfloat16))


def solution(mesh):
    placed = (
        P(("ep", "tp"), None),
        P(("ep", "tp"), None),
        P(),
        P(),
        P(),
        P("tp", None),
        P(("ep", "tp"), None),
        P(),
        P(("ep", "tp"), None),
        P(("ep", "tp"), None),
        P(("ep", "tp"), None, None),
        P(("ep", "tp"), None, None),
        P(("ep", "tp"), None, None),
    )
    return jax.shard_map(
        body,
        mesh=mesh,
        in_specs=placed,
        out_specs=(P(("ep", "tp"), None), P(("ep", "tp"), None)),
        check_vma=False,
    )
```

profile of v0, /device:TPU:1, one launch (start us, length us, event | category | flops | bytes accessed | tf_op | source)
XLA Modules:
  0.0 243.0 jit_solution(6507926595285209233)
XLA Ops:
  7.2 0.7 broadcast_multiply_fusion.1
  7.8 0.8 copy.20
  8.6 0.1 eq.29
  8.7 0.1 eq.25
  8.9 1.2 fusion.46
  10.1 0.1 copy.19
  10.2 0.1 mul.523
  10.3 0.1 copy.22
  10.4 0.2 fusion.57
  10.8 0.2 fusion.56
  11.0 2.4 %scatter_custom_fusion.1 = s32[640]{0:T(1024)S(1)} fusion(s32[512]{0:T(512)S(1)} %bitcast.135, s32[512]{0:T(512)S(1)} %iota.11, s32[]{:T(128)} %constant.17.clone.1), kind=kCustom, calls=%fused_computation.127 | custom fusion | bytes 2564 | tf_op jit(solution)/shard_map/scatter | solution.py:76
  13.5 1.2 fusion.48
  14.7 3.4 %gather_fusion = bf16[640,2048]{1,0:T(8,128)(2,1)S(1)} fusion(bf16[128,2048]{1,0:T(8,128)(2,1)S(1)} %fusion.48, s32[1024]{0:T(1024)S(1)} %pad_clamp_fusion.1), kind=kCustom, calls=%fused_computation | custom fusion | bytes 5245440 | tf_op jit(solution)/shard_map/gather | solution.py:80
  18.2 2.8 %gather.9 = bf16[128,5,2048]{2,1,0:T(8,128)(2,1)} reshape(bf16[640,2048]{1,0:T(8,128)(2,1)S(1)} %gather_fusion) | data formatting | bytes 5242880 | tf_op jit(solution)/shard_map/gather | solution.py:80
  21.0 2.4 %scatter_custom_fusion = pred[640]{0:T(1024)(128)(4,1)S(1)} fusion(s32[512]{0:T(512)S(1)} %bitcast.136, pred[512]{0:T(512)(128)(4,1)S(1)} %broadcast.104, pred[]{:T(512)} %constant.25.clone.1), kind=kCustom, calls=%fused_computation.130 | custom fusion | bytes 641 | tf_op jit(solution)/shard_map/scatter | solution.py:78
  23.4 0.2 broadcast_in_dim.36
  23.7 4.7 %broadcast_select_fusion = bf16[128,5,2048]{2,1,0:T(8,128)(2,1)} fusion(bf16[128,5,2048]{2,1,0:T(8,128)(2,1)} %gather.9, pred[128,5]{1,0:T(8,128)(4,1)S(1)} %broadcast_in_dim.36), kind=kLoop, calls=%fused_computation.74 | loop fusion | flops 1310720 | bytes 5243520 | tf_op jit(solution)/shard_map/jit(_where)/select_n | solution.py:79
  28.3 0.0 copy-start.1
  28.3 0.0 copy-start.2
  28.3 0.0 copy-start.3
  28.3 11.9 %all-to-all-start = ((bf16[128,5,2048]{2,1,0:T(8,128)(2,1)}), bf16[128,5,2048]{2,1,0:T(8,128)(2,1)}, u32[]{:S(2)}, u32[]{:S(2)}) async-start(bf16[128,5,2048]{2,1,0:T(8,128)(2,1)} %broadcast_select_fusion), calls=%async_computation | async-start | bytes 8388608 | tf_op jit(solution)/shard_map/all_to_all | solution.py:85
  40.3 0.0 all-gather.2.cloned.1.call-start
  40.3 0.7 all-gather.2.cloned.1.call-update
  41.0 0.0 copy-done.1
  41.0 0.9 slice_bitcast_fusion.2
  41.9 3.7 %collective-permute-start = (bf16[2,30,1024]{2,1,0:T(8,128)(2,1)S(1)}, bf16[2,30,1024]{2,1,0:T(8,128)(2,1)S(1)}, u32[]{:S(2)}, u32[]{:S(2)}) collective-permute-start(bf16[2,30,1024]{2,1,0:T(8,128)(2,1)S(1)} %pad_maximum_fusion), channel_id=1, source_target_pairs={{0,1},{1,2},{2,3},{3,4},{4,5},{5,6},{6,7},{7,8},{8,9},{9,10},{10,1... | collective-permute-start | bytes 368648 | tf_op jit(solution)/shard_map/ppermute | solution.py:13
  45.7 0.0 copy-done.2
  45.7 0.1 fusion.74
  45.8 0.0 copy-done.3
  45.8 50.1 %collective-permute-done = bf16[2,30,1024]{2,1,0:T(8,128)(2,1)S(1)} collective-permute-done((bf16[2,30,1024]{2,1,0:T(8,128)(2,1)S(1)}, bf16[2,30,1024]{2,1,0:T(8,128)(2,1)S(1)}, u32[]{:S(2)}, u32[]{:S(2)}) %collective-permute-start) | collective-permute-done | bytes 122912 | tf_op jit(solution)/shard_map/ppermute | solution.py:13
  96.0 4.2 %divide_multiply_fusion = f32[1054,1024]{1,0:T(8,128)} fusion(bf16[1024,1024]{1,0:T(8,128)(2,1)S(1)} %copy-done.1, bf16[30,1024]{1,0:T(8,128)(2,1)S(1)} %get-tuple-element.40, bf16[1024,1024]{1,0:T(8,128)(2,1)} %param.14, bf16[30,1024]{1,0:T(8,128)(2,1)S(1)} %get-tuple-element.39), kind=kLoop, calls=%fused_computation.4 | loop fusion | flops 12951552 | bytes 8634368 | tf_op jit(solution)/shard_map/mul | solution.py:46
  100.1 0.0 all-to-all-done
  100.1 4.2 %reshape.102 = bf16[640,2048]{1,0:T(8,128)(2,1)S(1)} reshape(bf16[128,5,2048]{2,1,0:T(8,128)(2,1)} %all-to-all-done) | data formatting | bytes 5242880 | tf_op jit(solution)/shard_map/reshape | solution.py:95
  104.3 6.6 %fusion.34 = f32[640,1024]{1,0:T(8,128)} fusion(bf16[640,2048]{1,0:T(8,128)(2,1)S(1)} %reshape.102, bf16[1,2048,1024]{2,1,0:T(8,128)(2,1)} %param.24), kind=kOutput, calls=%fused_computation.70 | convolution fusion | flops 2684354560 | bytes 9437184 | tf_op jit(solution)/shard_map/dot_general | solution.py:18
  110.9 11.9 %fusion.36 = bf16[640,2048]{1,0:T(8,128)(2,1)} fusion(bf16[1,1024,2048]{2,1,0:T(8,128)(2,1)} %param.25, f32[640,1024]{1,0:T(8,128)} %fusion.34, bf16[640,2048]{1,0:T(8,128)(2,1)S(1)} %reshape.102, bf16[1,2048,1024]{2,1,0:T(8,128)(2,1)} %param.23), kind=kOutput, calls=%fused_computation.76 | convolution fusion | flops 5376573440 | bytes 16252928 | tf_op jit(solution)/shard_map/dot_general | solution.py:22
  122.9 5.4 %reshape.103 = bf16[128,5,2048]{2,1,0:T(8,128)(2,1)} reshape(bf16[640,2048]{1,0:T(8,128)(2,1)} %fusion.36) | data formatting | bytes 5242880 | tf_op jit(solution)/shard_map/reshape | solution.py:97
  128.3 13.2 %all-to-all-start.1 = ((bf16[128,5,2048]{2,1,0:T(8,128)(2,1)}), bf16[128,5,2048]{2,1,0:T(8,128)(2,1)}, u32[]{:S(2)}, u32[]{:S(2)}) async-start(bf16[128,5,2048]{2,1,0:T(8,128)(2,1)} %reshape.103), calls=%async_computation.1 | async-start | bytes 8388608 | tf_op jit(solution)/shard_map/all_to_all | solution.py:98
  141.5 64.8 %fusion.71 = (f32[1024]{0:T(1024)S(1)}, f32[1024,1024]{1,0:T(8,128)S(1)}) fusion(f32[1054,1024]{1,0:T(8,128)} %divide_multiply_fusion, f32[1024]{0:T(1024)S(1)} %bitcast.112, f32[1024]{0:T(1024)S(1)} %bitcast.113, f32[1024]{0:T(1024)S(1)} %bitcast.115, f32[1024]{0:T(1024)S(1)} %bitcast.116, f32[1024]{0:T(1024)S(1)} %bitcast.117, f32[1024]{0:T(1024)S(1)} %bitcast.118, ...), kind=kLoop, calls=%fused_computation.143 | loop fusion | flops 65010688 | bytes 134348800 | tf_op jit(solution)/shard_map/reduce_sum | solution.py:50
  206.3 0.0 copy-start
  206.3 1.9 copy-done
  208.2 0.6 multiply_reduce_fusion
  208.8 0.0 all-to-all-done.1
  208.8 4.2 %reshape.104 = bf16[640,2048]{1,0:T(8,128)(2,1)S(1)} reshape(bf16[128,5,2048]{2,1,0:T(8,128)(2,1)} %all-to-all-done.1) | data formatting | bytes 5242880 | tf_op jit(solution)/shard_map/reshape | solution.py:99
  213.0 3.3 %gather_fusion.1 = bf16[512,2048]{1,0:T(8,128)(2,1)} fusion(bf16[640,2048]{1,0:T(8,128)(2,1)S(1)} %reshape.104, s32[1024]{0:T(1024)S(1)} %pad_clamp_fusion), kind=kCustom, calls=%fused_computation.1 | custom fusion | bytes 4196352 | tf_op jit(solution)/shard_map/gather | solution.py:99
  216.3 2.7 %reshape.105 = bf16[128,4,2048]{2,1,0:T(4,128)(2,1)S(1)} reshape(bf16[512,2048]{1,0:T(8,128)(2,1)} %gather_fusion.1) | data formatting | bytes 4194304 | tf_op jit(solution)/shard_map/reshape | solution.py:99
  219.0 3.3 %fusion.73 = (bf16[128,1,2048]{2,1,0:T(2,128)(2,1)S(1)}, bf16[128,1,2048]{2,1,0:T(2,128)(2,1)S(1)}, bf16[128,1,2048]{2,1,0:T(2,128)(2,1)S(1)}, bf16[128,1,2048]{2,1,0:T(2,128)(2,1)S(1)}) fusion(bf16[128,4,2048]{2,1,0:T(4,128)(2,1)S(1)} %reshape.105), kind=kLoop, calls=%fused_computation.144 | loop fusion | bytes 4194304 | tf_op jit(solution)/shard_map/slice | solution.py:104
  222.4 0.0 copy-start.4
  222.4 0.0 copy-start.5
  222.4 3.0 %fusion.50 = bf16[128,2048]{1,0:T(8,128)(2,1)} fusion(bf16[128,1,2048]{2,1,0:T(2,128)(2,1)S(1)} %get-tuple-element.7, bf16[128,1,2048]{2,1,0:T(2,128)(2,1)S(1)} %get-tuple-element.5, bf16[128,1,2048]{2,1,0:T(2,128)(2,1)S(1)} %get-tuple-element.6, bf16[128,1,2048]{2,1,0:T(2,128)(2,1)S(1)} %get-tuple-element.4, f32[128]{0:T(128)S(1)} %get-tuple-element.43, ...), kind=kLoop, calls=%fused_computation.90 | loop fusion | flops 3145728 | bytes 2623488 | tf_op jit(solution)/shard_map/convert_element_type | solution.py:107
  225.4 0.0 all-gather.2.cloned.1.call-done
  225.4 0.0 copy-done.4
  225.4 0.0 copy-done.5
  225.4 10.7 %convolution_convert_fusion = bf16[1024,2048]{1,0:T(8,128)(2,1)} fusion(bf16[1024,2048]{1,0:T(8,128)(2,1)} %all-gather.2.cloned.1.call-done, f32[1024,1024]{1,0:T(8,128)} %copy-done, f32[1024]{0:T(1024)S(1)} %copy-done.4, f32[1024]{0:T(1024)S(1)} %copy-done.5, f32[1024]{0:T(1024)S(1)} %add_rsqrt_fusion, f32[1024]{0:T(1024)S(1)} %broadcast_multiply_fusion), kind=kOutput, calls=%fused_computation.75 | convolution fusion | flops 4306501632 | bytes 12599296 | tf_op jit(solution)/shard_map/dot_general | solution.py:54
  (19 shorter events, 0.2 us)
Async XLA Ops:
  28.3 12.7 %copy-start.1 = (bf16[1024,1024]{1,0:T(8,128)(2,1)S(1)}, bf16[1024,1024]{1,0:T(8,128)(2,1)}, u32[]{:S(2)}) copy-start(bf16[1024,1024]{1,0:T(8,128)(2,1)} %param.13) | copy-start | bytes 6291460
  28.3 17.3 %copy-start.2 = (f32[31,1024]{1,0:T(8,128)S(1)}, f32[31,1024]{1,0:T(8,128)}, u32[]{:S(2)}) copy-start(f32[31,1024]{1,0:T(8,128)} %param.15) | copy-start | bytes 380932
  28.3 17.5 %copy-start.3 = (f32[128,4]{0,1:T(4,128)S(1)}, f32[128,4]{0,1:T(4,128)}, u32[]{:S(2)}) copy-start(f32[128,4]{0,1:T(4,128)} %param.22) | copy-start | bytes 6148
  28.3 71.8 %all-to-all-start = ((bf16[128,5,2048]{2,1,0:T(8,128)(2,1)}), bf16[128,5,2048]{2,1,0:T(8,128)(2,1)}, u32[]{:S(2)}, u32[]{:S(2)}) async-start(bf16[128,5,2048]{2,1,0:T(8,128)(2,1)} %broadcast_select_fusion), calls=%async_computation | async-start | bytes 8388608 | tf_op jit(solution)/shard_map/all_to_all | solution.py:85
  40.3 185.1 %all-gather.2.cloned.1.call-start = ((), (), s32[]{:S(2)}) async-start(), calls=%async_computation.2 | async-start | bytes 4718592 | tf_op jit(solution)/shard_map/all_gather | solution.py:56
  41.9 54.0 %collective-permute-start = (bf16[2,30,1024]{2,1,0:T(8,128)(2,1)S(1)}, bf16[2,30,1024]{2,1,0:T(8,128)(2,1)S(1)}, u32[]{:S(2)}, u32[]{:S(2)}) collective-permute-start(bf16[2,30,1024]{2,1,0:T(8,128)(2,1)S(1)} %pad_maximum_fusion), channel_id=1, source_target_pairs={{0,1},{1,2},{2,3},{3,4},{4,5},{5,6},{6,7},{7,8},{8,9},{9,10},{10,1... | collective-permute-start | bytes 368648 | tf_op jit(solution)/shard_map/ppermute | solution.py:13
  128.3 80.5 %all-to-all-start.1 = ((bf16[128,5,2048]{2,1,0:T(8,128)(2,1)}), bf16[128,5,2048]{2,1,0:T(8,128)(2,1)}, u32[]{:S(2)}, u32[]{:S(2)}) async-start(bf16[128,5,2048]{2,1,0:T(8,128)(2,1)} %reshape.103), calls=%async_computation.1 | async-start | bytes 8388608 | tf_op jit(solution)/shard_map/all_to_all | solution.py:98
  206.3 1.9 copy-start
  222.4 3.0 %copy-start.4 = (f32[1024]{0:T(1024)S(1)}, f32[1024]{0:T(1024)}, u32[]{:S(2)}) copy-start(f32[1024]{0:T(1024)} %param.17) | copy-start | bytes 12292
  222.4 3.0 %copy-start.5 = (f32[1024]{0:T(1024)S(1)}, f32[1024]{0:T(1024)}, u32[]{:S(2)}) copy-start(f32[1024]{0:T(1024)} %param.16) | copy-start | bytes 12292
Sparse Core Ops, SparseCore 0:
  42.8 65.1 all-gather.1
where the time goes:
time: 244 us; the launch traced here: 243 us
  other arithmetic  80.9 us (33%)
  waiting for transfers between devices  50.8 us (21%)
  local copies, waits for them, and re-layouts  38.8 us (16%)
  matrix products  29.2 us (12%)
  starting transfers between devices  28.9 us (12%)
  between operations  14.3 us (6%)
    reduce_sum x1, other arithmetic, body(): center = jnp.mean(convolved, axis=-1, keepdims=True)  64.8 us
    ppermute x1, waiting for transfers between devices, passed_along(): lax.ppermute(value, axis, [(source, source + steps) for source in range(f...  50.1 us
    all_to_all x1, starting transfers between devices, body(): lax.all_to_all(answers, ('ep', 'tp'), split_axis=0, concat_axis=0, tiled=...  13.2 us
    all_to_all x1, starting transfers between devices, body(): lax.all_to_all(outgoing.reshape(experts, capacity, model_width), ('ep', '...  11.9 us
    dot_general x1, matrix products, expert_apply(): jnp.dot(hidden, down_matrix, preferred_element_type=jnp.float32)  11.9 us
    dot_general x1, matrix products, body(): jnp.dot(activated, lax.all_gather(mix_out_weight, 'tp', axis=0, tiled=Tru...  10.7 us
    reshape x2, local copies, waits for them, and re-layouts, body(): returned.reshape(experts * capacity, model_width)[slot_index]  6.92 us
    dot_general x1, matrix products, expert_apply(): pre_up = jnp.dot(flat_rows, up_matrix, preferred_element_type=jnp.float32)  6.59 us
  transfers between devices with their start and end apart: 4, of which 1 were waited for; matrix products, arithmetic and copies ran while one was open for 47% of the time, Pallas kernels for 0%

commit v1 on v0

v1 whole, which is shorter than its diff:
```python
import functools

import jax
import jax.numpy as jnp
from jax import lax
from jax.experimental import pallas as pl
from jax.experimental.pallas import tpu as pltpu
from jax.sharding import PartitionSpec as P

MESH = pl.DeviceIdType.MESH
F32 = jnp.float32
BF16 = jnp.bfloat16
CLAMP_LIMIT = 7.0
GLU_SLOPE = 1.702
CAP = 5
PEERS = 128
SCRAMBLE = 101
GROUPS = 4
GSIZE = PEERS // GROUPS
PIECES = 16
BLOCK = CAP * PIECES
PITCH = 88
HALO = 32
SEGMENT = 129
CONV_STEP = 12
CONV_BLOCKS = -(-SEGMENT // CONV_STEP)


def sigmoid(v):
    return 0.5 + 0.5 * jnp.tanh(0.5 * v)


def displacement(i):
    j = (i * SCRAMBLE) % PEERS
    return j // 32, (j // 8) % 4, (j // 2) % 4, j % 2


def kernel(
    value_hbm, gate_hbm, taps_ref, cgain_ref, cshift_ref, wout_hbm, moe_hbm, mgain_ref, ids_ref, share_ref,
    wg_hbm, wu_hbm, wd_hbm,
    mixed_hbm, moe_out_hbm,
    value, gate, halo, glu, conv, act, wfull, obuf,
    xin, xn, rankm, sharem, sbuf, abuf, rbuf, tbuf, scr, rows, hidden, wg, wu, wd, result, mout,
    local_sem, out_sem, halo_send, halo_recv, w_send, w_recv, wf_send, wf_recv,
    d_send, d_recv, r_send, r_recv, self_sem,
):
    ep = lax.axis_index("ep")
    tp = lax.axis_index("tp")
    me = ep * 8 + tp
    z, x, y, c = ep // 4, ep % 4, tp // 2, tp % 2

    def device(dz, dx, dy, dc):
        return ((z + dz + 4) % 4) * 4 + (x + dx + 4) % 4, ((y + dy + 4) % 4) * 2 + (c + dc) % 2

    barrier = pltpu.get_barrier_semaphore()

    def hello(i, carry):
        target = device(*displacement(i))
        pl.semaphore_signal(barrier, inc=1, device_id=target, device_id_type=MESH)
        return carry

    lax.fori_loop(1, PEERS, hello, 0)

    load_moe = pltpu.make_async_copy(moe_hbm, xin, local_sem.at[0])
    load_w = pltpu.make_async_copy(wout_hbm, wfull.at[pl.ds(pl.multiple_of(tp * 128, 128), 128), :], local_sem.at[1])
    load_value = pltpu.make_async_copy(value_hbm, value, local_sem.at[2])
    load_gate = pltpu.make_async_copy(gate_hbm, gate, local_sem.at[3])
    load_wg = pltpu.make_async_copy(wg_hbm.at[0], wg, local_sem.at[4])
    load_wu = pltpu.make_async_copy(wu_hbm.at[0], wu, local_sem.at[5])
    load_wd = pltpu.make_async_copy(wd_hbm.at[0], wd, local_sem.at[6])
    for load in (load_moe, load_value, load_gate, load_w, load_wg, load_wu, load_wd):
        load.start()

    lane = lax.broadcasted_iota(jnp.int32, (128, PEERS), 1)
    row = lax.broadcasted_iota(jnp.int32, (128, PEERS), 0)
    j = (lane * SCRAMBLE) & 127
    expert = (
        (((z + (j >> 5)) & 3) * 32) + (((x + (j >> 3)) & 3) * 8) + (((y + (j >> 1)) & 3) * 2) + ((c + j) & 1)
    )
    chosen = jnp.zeros((128, PEERS), F32)
    shares = jnp.zeros((128, PEERS), F32)
    for k in range(4):
        hit = ids_ref[:, k : k + 1] == expert
        chosen = jnp.where(hit, 1.0, chosen)
        shares = jnp.where(hit, share_ref[:, k : k + 1], shares)
    before = jnp.where(row > lane, 1.0, 0.0).astype(BF16)
    rank = jnp.dot(before, chosen.astype(BF16), preferred_element_type=F32)
    rankm[...] = jnp.where(chosen > 0.5, rank, -1.0)
    sharem[...] = shares

    load_moe.wait()

    def norm_rows(b, carry):
        at = pl.ds(pl.multiple_of(b * 32, 32), 32)
        f = xin[at, :].astype(F32)
        scaled = f * lax.rsqrt(jnp.mean(f * f, axis=-1, keepdims=True) + 1e-06)
        xn[at, :] = (scaled * mgain_ref[...]).astype(BF16)
        return carry

    lax.fori_loop(0, 4, norm_rows, 0)

    def pack(dst, first):
        def one(i, carry):
            dst[first + i] = scr[pl.ds(pl.multiple_of(i * PITCH, 8), BLOCK), :].astype(BF16)
            return carry

        lax.fori_loop(0, GSIZE, one, 0, unroll=4)

    def unpack(src, first):
        def one(i, carry):
            scr[pl.ds(pl.multiple_of(i * PITCH, 8), BLOCK), :] = src[first + i].astype(F32)
            return carry

        lax.fori_loop(0, GSIZE, one, 0, unroll=4)

    def gather(g):
        for r in range(CAP):
            take = jnp.where(rankm[...] == float(r), 1.0, 0.0).astype(BF16)[:, g * GSIZE : (g + 1) * GSIZE]

            def some(n, carry, take=take, r=r):
                cols = pl.ds(pl.multiple_of(n * 512, 512), 512)
                got = lax.dot_general(take, xn[:, cols], (((0,), (0,)), ((), ())), preferred_element_type=F32)
                for q in range(4):
                    scr[pl.ds(r * PIECES + n * 4 + q, GSIZE, stride=PITCH), :] = got[:, q * 128 : (q + 1) * 128]
                return carry

            lax.fori_loop(0, 4, some, 0)
        pack(sbuf, g * GSIZE)

    def send_group(g):
        def one(i, carry):
            pltpu.make_async_remote_copy(
                src_ref=sbuf.at[i], dst_ref=abuf.at[i], send_sem=d_send, recv_sem=d_recv.at[g],
                device_id=device(*displacement(i)), device_id_type=MESH,
            ).start()
            return carry

        lax.fori_loop(max(1, g * GSIZE), (g + 1) * GSIZE, one, 0)

    gather(0)
    load_value.wait()
    load_gate.wait()
    load_w.wait()
    pl.semaphore_wait(barrier, PEERS - 1)

    nxt = (me + 1) % 128
    halo_copies = []
    for n, half in enumerate((value, gate)):
        cp = pltpu.make_async_remote_copy(
            src_ref=half.at[pl.ds(1024 - HALO, HALO), :], dst_ref=halo.at[n],
            send_sem=halo_send.at[n], recv_sem=halo_recv.at[n],
            device_id=(nxt // 8, nxt % 8), device_id_type=MESH,
        )
        cp.start()
        halo_copies.append(cp)
    self_copy = pltpu.make_async_copy(sbuf.at[0], abuf.at[0], self_sem.at[0])
    self_copy.start()
    send_group(0)
    for g in range(1, GROUPS):
        gather(g)
        send_group(g)

    mine = wfull.at[pl.ds(pl.multiple_of(tp * 128, 128), 128), :]
    w_copies = []
    for d in range(1, 4):
        cp = pltpu.make_async_remote_copy(
            src_ref=mine, dst_ref=mine, send_sem=w_send.at[d - 1], recv_sem=w_recv.at[d - 1],
            device_id=device(0, 0, d, 0), device_id_type=MESH,
        )
        cp.start()
        w_copies.append(cp)
    wf_copies = []

    def forward(d):
        origin = ((y - d + 4) % 4) * 2 + c
        block = wfull.at[pl.ds(pl.multiple_of(origin * 128, 128), 128), :]
        cp = pltpu.make_async_remote_copy(
            src_ref=block, dst_ref=block, send_sem=wf_send.at[d], recv_sem=wf_recv.at[d],
            device_id=device(0, 0, 0, 1), device_id_type=MESH,
        )
        cp.start()
        wf_copies.append(cp)

    forward(0)

    def glu_rows(b, carry):
        at = pl.ds(pl.multiple_of(b * 32, 32), 32)
        to = pl.ds(pl.multiple_of(b * 32 + HALO, 32), 32)
        gated = value[at, :].astype(F32) * sigmoid(gate[at, :].astype(F32))
        for l in range(8):
            glu[l, to, :] = gated[:, l * 128 : (l + 1) * 128]
        return carry

    lax.fori_loop(0, 1024 // 32, glu_rows, 0)
    for cp in halo_copies:
        cp.wait()
    border = halo[0].astype(F32) * sigmoid(halo[1].astype(F32))
    border = border * jnp.minimum(me, 1).astype(F32)
    for l in range(8):
        glu[l, pl.ds(0, HALO), :] = border[:, l * 128 : (l + 1) * 128]
        glu[l, pl.ds(1024 + HALO, 8), :] = jnp.zeros((8, 128), F32)

    def conv_block(n, carry):
        l, block = n // CONV_BLOCKS, n % CONV_BLOCKS
        lanes = pl.ds(pl.multiple_of(l * 128, 128), 128)
        b0 = jnp.minimum(block * CONV_STEP, SEGMENT - CONV_STEP)
        near = [glu[l, pl.ds(b0 + 2 + u, 8, stride=SEGMENT), :] for u in range(CONV_STEP + 30)]
        totals = [None] * CONV_STEP
        for tap in range(31):
            w = jnp.broadcast_to(taps_ref[tap : tap + 1, lanes], (8, 128))
            for b in range(CONV_STEP):
                term = w * near[b + tap]
                totals[b] = term if tap == 0 else totals[b] + term
        for b in range(CONV_STEP):
            conv[l, pl.ds(b0 + b, 8, stride=SEGMENT), :] = totals[b]
        return carry

    lax.fori_loop(0, 8 * CONV_BLOCKS, conv_block, 0)

    def norm_conv(n, carry):
        at = pl.ds(pl.multiple_of(n * 32, 32), 32)
        v = jnp.concatenate([conv[l, at, :] for l in range(8)], axis=-1)
        center = jnp.mean(v, axis=-1, keepdims=True)
        v = v - center
        spread = jnp.mean(v * v, axis=-1, keepdims=True)
        u = v * lax.rsqrt(spread + 1e-05) * cgain_ref[...] + cshift_ref[...]
        act[at, :] = (u * sigmoid(u)).astype(BF16)
        return carry

    lax.fori_loop(0, 32, norm_conv, 0, unroll=2)

    load_wg.wait()
    load_wu.wait()
    load_wd.wait()

    def group_wait(buf, sem, g):
        n = GSIZE - 1 if g == 0 else GSIZE
        pltpu.make_async_copy(buf.at[pl.ds(0, n)], buf.at[pl.ds(0, n)], sem.at[g]).wait()

    def experts(g):
        unpack(abuf, g * GSIZE)

        def line_up(n, carry):
            cols = pl.ds(pl.multiple_of(n * 128, 128), 128)
            for r in range(CAP):
                rows[pl.ds(r * GSIZE, GSIZE), cols] = scr[pl.ds(r * PIECES + n, GSIZE, stride=PITCH), :].astype(BF16)
            return carry

        lax.fori_loop(0, PIECES, line_up, 0)

        def up(n, carry):
            cols = pl.ds(pl.multiple_of(n * 256, 256), 256)
            pre_gate = jnp.dot(rows[...], wg[:, cols], preferred_element_type=F32)
            pre_up = jnp.dot(rows[...], wu[:, cols], preferred_element_type=F32)
            gated = jnp.minimum(pre_gate, CLAMP_LIMIT)
            lifted = jnp.clip(pre_up, -CLAMP_LIMIT, CLAMP_LIMIT) + 1.0
            hidden[:, cols] = (lifted * gated * sigmoid(GLU_SLOPE * gated)).astype(BF16)
            return carry

        lax.fori_loop(0, 4, up, 0)

        def down(n, carry):
            cols = pl.ds(pl.multiple_of(n * 256, 256), 256)
            got = jnp.dot(hidden[...], wd[:, cols], preferred_element_type=F32)
            for r in range(CAP):
                for q in range(2):
                    scr[pl.ds(r * PIECES + n * 2 + q, GSIZE, stride=PITCH), :] = got[
                        r * GSIZE : (r + 1) * GSIZE, q * 128 : (q + 1) * 128
                    ]
            return carry

        lax.fori_loop(0, 8, down, 0)
        pack(rbuf, g * GSIZE)

        def give_back(i, carry):
            dz, dx, dy, dc = displacement(i)
            pltpu.make_async_remote_copy(
                src_ref=rbuf.at[i], dst_ref=tbuf.at[i], send_sem=r_send, recv_sem=r_recv.at[g],
                device_id=device(-dz, -dx, -dy, dc), device_id_type=MESH,
            ).start()
            return carry

        lax.fori_loop(max(1, g * GSIZE), (g + 1) * GSIZE, give_back, 0)

    self_copy.wait()
    for g in range(GROUPS):
        group_wait(abuf, d_recv, g)
        experts(g)
    self_back = pltpu.make_async_copy(rbuf.at[0], tbuf.at[0], self_sem.at[1])
    self_back.start()

    for d in range(1, 4):
        w_copies[d - 1].wait()
        forward(d)
    for cp in wf_copies:
        cp.wait()

    def project(m, carry):
        at = pl.ds(pl.multiple_of(m * 256, 256), 256)

        def part(n, inner):
            cols = pl.ds(pl.multiple_of(n * 512, 512), 512)
            obuf[at, cols] = jnp.dot(act[at, :], wfull[:, cols], preferred_element_type=F32).astype(BF16)
            return inner

        lax.fori_loop(0, 4, part, 0)
        return carry

    lax.fori_loop(0, 4, project, 0)
    store_mixed = pltpu.make_async_copy(obuf, mixed_hbm, out_sem.at[0])
    store_mixed.start()

    self_back.wait()
    for g in range(GROUPS):
        group_wait(tbuf, r_recv, g)
        unpack(tbuf, g * GSIZE)

        def line_up_back(n, carry, g=g):
            cols = pl.ds(pl.multiple_of(n * 128, 128), 128)
            for r in range(CAP):
                result[pl.ds(r * PEERS + g * GSIZE, GSIZE), cols] = scr[
                    pl.ds(r * PIECES + n, GSIZE, stride=PITCH), :
                ].astype(BF16)
            return carry

        lax.fori_loop(0, PIECES, line_up_back, 0)
    weights = jnp.concatenate(
        [jnp.where(rankm[...] == float(r), sharem[...], 0.0).astype(BF16) for r in range(CAP)], axis=1
    )

    def combine(n, carry):
        cols = pl.ds(pl.multiple_of(n * 512, 512), 512)
        mout[:, cols] = jnp.dot(weights, result[:, cols], preferred_element_type=F32).astype(BF16)
        return carry

    lax.fori_loop(0, 4, combine, 0)
    store_moe = pltpu.make_async_copy(mout, moe_out_hbm, out_sem.at[1])
    store_moe.start()
    sent = sbuf.at[pl.ds(0, PEERS - 1)]
    pltpu.make_async_copy(sent, sent, d_send).wait()
    pltpu.make_async_copy(sent, sent, r_send).wait()
    store_mixed.wait()
    store_moe.wait()


def body(
    glu_value, glu_gate, conv_taps, chan_gain, chan_shift, mix_out_weight, moe_input, moe_gain, expert_ids,
    expert_share, expert_gate_weight, expert_up_weight, expert_down_weight,
):
    hbm = pl.BlockSpec(memory_space=pl.ANY)
    vmem = pl.BlockSpec(memory_space=pltpu.VMEM)
    dma = pltpu.SemaphoreType.DMA
    return pl.pallas_call(
        kernel,
        out_shape=(
            jax.ShapeDtypeStruct((1024, 2048), BF16),
            jax.ShapeDtypeStruct((128, 2048), BF16),
        ),
        in_specs=[hbm, hbm, vmem, vmem, vmem, hbm, hbm, vmem, vmem, vmem, hbm, hbm, hbm],
        out_specs=(hbm, hbm),
        scratch_shapes=[
            pltpu.VMEM((1024, 1024), BF16),
            pltpu.VMEM((1024, 1024), BF16),
            pltpu.VMEM((2, HALO, 1024), BF16),
            pltpu.VMEM((8, 1024 + HALO + 8, 128), F32),
            pltpu.VMEM((8, 8 * SEGMENT, 128), F32),
            pltpu.VMEM((1024, 1024), BF16),
            pltpu.VMEM((1024, 2048), BF16),
            pltpu.VMEM((1024, 2048), BF16),
            pltpu.VMEM((128, 2048), BF16),
            pltpu.VMEM((128, 2048), BF16),
            pltpu.VMEM((128, PEERS), F32),
            pltpu.VMEM((128, PEERS), F32),
            pltpu.VMEM((PEERS, BLOCK, 128), BF16),
            pltpu.VMEM((PEERS, BLOCK, 128), BF16),
            pltpu.VMEM((PEERS, BLOCK, 128), BF16),
            pltpu.VMEM((PEERS, BLOCK, 128), BF16),
            pltpu.VMEM((GSIZE * PITCH, 128), F32),
            pltpu.VMEM((GSIZE * CAP, 2048), BF16),
            pltpu.VMEM((GSIZE * CAP, 1024), BF16),
            pltpu.VMEM((2048, 1024), BF16),
            pltpu.VMEM((2048, 1024), BF16),
            pltpu.VMEM((1024, 2048), BF16),
            pltpu.VMEM((PEERS * CAP, 2048), BF16),
            pltpu.VMEM((128, 2048), BF16),
            dma((7,)), dma((2,)), dma((2,)), dma((2,)), dma((3,)), dma((3,)), dma((4,)), dma((4,)),
            dma, dma((GROUPS,)), dma, dma((GROUPS,)), dma((2,)),
        ],
        compiler_params=pltpu.CompilerParams(
            collective_id=0, has_side_effects=True, vmem_limit_bytes=62 * 2**20
        ),
        name="mixer",
    )(
        glu_value, glu_gate, conv_taps, chan_gain.reshape(1, -1), chan_shift.reshape(1, -1), mix_out_weight,
        moe_input, moe_gain.reshape(1, -1), expert_ids, expert_share,
        expert_gate_weight, expert_up_weight, expert_down_weight,
    )


def solution(mesh):
    both = ("ep", "tp")
    placed = (
        P(both, None), P(both, None), P(), P(), P(), P("tp", None), P(both, None), P(), P(both, None),
        P(both, None), P(both, None, None), P(both, None, None), P(both, None, None),
    )
    return jax.shard_map(
        body,
        mesh=mesh,
        in_specs=placed,
        out_specs=(P(both, None), P(both, None)),
        check_vma=False,
    )
```

time: 244 us -> 115 us (0.47)
  Pallas kernels: 0 us -> 105 us
  other arithmetic: 80.9 us -> 0 us
  waiting for transfers between devices: 50.8 us -> 0 us
  local copies, waits for them, and re-layouts: 38.8 us -> 8.47 us
  matrix products: 29.2 us -> 0 us
  starting transfers between devices: 28.9 us -> 0 us
  between operations: 14.3 us -> 0.65 us
    pallas_call x0 -> x1, Pallas kernels: none -> 105 us  [body(): pl.pallas_call(kernel, out_shape=(jax.ShapeDtypeStruct((1024, 2048), BF16...]
    reduce_sum x4 -> x0, other arithmetic: 66.8 us -> none  [the longest x1 64.8 us: body(): center = jnp.mean(convolved, axis=-1, keepdims=True)]
    ppermute x1 -> x0, waiting for transfers between devices: 50.1 us -> none  [passed_along(): lax.ppermute(value, axis, [(source, source + steps) for source in range(f...]
    dot_general x3 -> x0, matrix products: 29.2 us -> none  [the longest x1 11.9 us: expert_apply(): jnp.dot(hidden, down_matrix, preferred_element_type=jnp.float32)]
    all_to_all x2 -> x0, starting transfers between devices: 25.2 us -> none  [the longest x1 13.2 us: body(): lax.all_to_all(answers, ('ep', 'tp'), split_axis=0, concat_axis=0, tiled=...]
    reshape x4 -> x0, local copies, waits for them, and re-layouts: 16.6 us -> none  [the longest x2 6.92 us: body(): returned.reshape(experts * capacity, model_width)[slot_index]]
    gather x3 -> x0, local copies, waits for them, and re-layouts: 9.52 us -> none  [the longest x2 6.23 us: body(): moe_normed[slot_owner // per_token]]
    unnamed x14 -> x6, local copies, waits for them, and re-layouts: 2.72 us -> 8.47 us
  transfers between devices with their start and end apart: 4 -> 0, of which waited for: 1 -> 0; matrix products, arithmetic and copies ran while one was open for 47% -> 0% of each run, Pallas kernels for 0% -> 0%
where the time goes in v1:
time: 115 us
  Pallas kernels  105 us (91%)
  local copies, waits for them, and re-layouts  8.47 us (7%)
    pallas_call x1, Pallas kernels, body(): pl.pallas_call(kernel, out_shape=(jax.ShapeDtypeStruct((1024, 2048), BF16...  105 us
    unnamed x6, local copies, waits for them, and re-layouts  8.47 us

profile of v1, /device:TPU:1, one launch (start us, length us, event | category | flops | bytes accessed | tf_op | source)
XLA Modules:
  0.0 114.5 jit_solution(15880863135179869730)
XLA Ops:
  0.6 1.4 %copy.15.ids_ref = s32[128,4]{1,0:T(8,128)} copy(s32[128,4]{0,1:T(4,128)} %param.21) | data formatting | bytes 4096 | tf_op args[8]
  2.0 1.4 %copy.16.share_ref = f32[128,4]{1,0:T(8,128)} copy(f32[128,4]{0,1:T(4,128)} %param.22) | data formatting | bytes 4096 | tf_op args[9]
  3.5 105.4 %mixer.1 = (bf16[1024,2048]{1,0:T(8,128)(2,1)}, bf16[128,2048]{1,0:T(8,128)(2,1)}) custom-call(bf16[1024,1024]{1,0:T(8,128)(2,1)} %value_hbm.1, bf16[1024,1024]{1,0:T(8,128)(2,1)} %gate_hbm.1, f32[31,1024]{1,0:T(8,128)} %taps_ref.1, f32[1,1024]{1,0:T(1,128)} %bitcast.4, f32[1,1024]{1,0:T(1,128)} %bitcast.5, bf16[128,2048]{1,0:T(8,128)(2,1)} %wout_hbm.1, ...), custom_call_target="tpu_custom_call" | custom-call | tf_op jit(solution)/shard_map/mixer/pallas_call | solution.py:353
  108.9 0.0 copy-start
  108.9 4.8 %copy.19 = bf16[1024,2048]{1,0:T(8,128)(2,1)} copy(bf16[1024,2048]{1,0:T(8,128)(2,1)} %get-tuple-element.4) | data formatting | bytes 8388608
  113.7 0.0 copy-done
  113.7 0.8 copy.20
Async XLA Ops:
  108.9 4.9 %copy-start = (bf16[128,2048]{1,0:T(8,128)(2,1)S(1)}, bf16[128,2048]{1,0:T(8,128)(2,1)}, u32[]{:S(2)}) copy-start(bf16[128,2048]{1,0:T(8,128)(2,1)} %get-tuple-element.5) | copy-start | bytes 1572868

commit v2 on v1

v2 whole, which is shorter than its diff:
```python
import functools

import jax
import jax.numpy as jnp
from jax import lax
from jax.experimental import pallas as pl
from jax.experimental.pallas import tpu as pltpu
from jax.sharding import PartitionSpec as P

MESH = pl.DeviceIdType.MESH
F32 = jnp.float32
BF16 = jnp.bfloat16
CLAMP_LIMIT = 7.0
GLU_SLOPE = 1.702
CAP = 5
PEERS = 128
SCRAMBLE = 101
GROUPS = 4
GSIZE = PEERS // GROUPS
PIECES = 16
BLOCK = CAP * PIECES
PITCH = 88
HALO = 32
SEGMENT = 129
CONV_STEP = 12
CONV_BLOCKS = -(-SEGMENT // CONV_STEP)


def sigmoid(v):
    return 0.5 + 0.5 * jnp.tanh(0.5 * v)


def displacement(i):
    j = (i * SCRAMBLE) & (PEERS - 1)
    return j >> 5, j >> 3, j >> 1, j


def kernel(
    value_hbm, gate_hbm, taps_hbm, cgain_hbm, cshift_hbm, wout_hbm, moe_hbm, mgain_hbm, ids_hbm, share_hbm,
    wg_hbm, wu_hbm, wd_hbm,
    mixed_hbm, moe_out_hbm,
    taps_ref, cgain_ref, cshift_ref, mgain_ref, ids_ref, share_ref, value, gate, halo, glu, conv, act, wfull, obuf,
    xin, xn, rankm, sharem, sbuf, abuf, rbuf, tbuf, scr, rows, hidden, wg, wu, wd, result, weights, mout,
    local_sem, out_sem, halo_send, halo_recv, w_send, w_recv, own_send, own_recv,
    d_send, d_recv, r_send, r_recv, self_sem,
):
    ep = lax.axis_index("ep")
    tp = lax.axis_index("tp")
    me = ep * 8 + tp
    z, x, y, c = ep >> 2, ep & 3, tp >> 1, tp & 1

    def device(dz, dx, dy, dc):
        return ((z + dz) & 3) * 4 + ((x + dx) & 3), ((y + dy) & 3) * 2 + ((c + dc) & 1)

    barrier = pltpu.get_barrier_semaphore()

    def hello(i, carry):
        pl.semaphore_signal(barrier, inc=1, device_id=device(*displacement(i)), device_id_type=MESH)
        return carry

    lax.fori_loop(1, PEERS, hello, 0, unroll=3)

    shard = pl.ds(pl.multiple_of(tp * 128, 128), 128)
    pairs = (
        (ids_hbm, ids_ref), (share_hbm, share_ref), (mgain_hbm, mgain_ref),
        (taps_hbm, taps_ref), (cgain_hbm, cgain_ref), (cshift_hbm, cshift_ref),
    )
    small = [pltpu.make_async_copy(a, b, local_sem.at[15 + n]) for n, (a, b) in enumerate(pairs)]
    load_moe = pltpu.make_async_copy(moe_hbm, xin, local_sem.at[0])
    load_w = [
        pltpu.make_async_copy(wout_hbm.at[:, pl.ds(n * 256, 256)], wfull.at[n, shard, :], local_sem.at[7 + n])
        for n in range(8)
    ]
    load_value = pltpu.make_async_copy(value_hbm, value, local_sem.at[2])
    load_gate = pltpu.make_async_copy(gate_hbm, gate, local_sem.at[3])
    load_wg = pltpu.make_async_copy(wg_hbm.at[0], wg, local_sem.at[4])
    load_wu = pltpu.make_async_copy(wu_hbm.at[0], wu, local_sem.at[5])
    load_wd = pltpu.make_async_copy(wd_hbm.at[0], wd, local_sem.at[6])
    for load in (*small, load_moe, *load_w, load_value, load_gate, load_wg, load_wu, load_wd):
        load.start()

    for load in small:
        load.wait()

    lane = lax.broadcasted_iota(jnp.int32, (PEERS, 128), 1)
    row = lax.broadcasted_iota(jnp.int32, (PEERS, 128), 0)
    j = (row * SCRAMBLE) & 127
    expert = (
        (((z + (j >> 5)) & 3) * 32) + (((x + (j >> 3)) & 3) * 8) + (((y + (j >> 1)) & 3) * 2) + ((c + j) & 1)
    )
    chosen = jnp.zeros((PEERS, 128), F32)
    shares = jnp.zeros((PEERS, 128), F32)
    for k in range(4):
        hit = ids_ref[k : k + 1, :] == expert
        chosen = jnp.where(hit, 1.0, chosen)
        shares = jnp.where(hit, share_ref[k : k + 1, :], shares)
    before = jnp.where(row < lane, 1.0, 0.0).astype(BF16)
    rank = jnp.dot(chosen.astype(BF16), before, preferred_element_type=F32)
    rankm[...] = jnp.where(chosen > 0.5, rank, -1.0)
    sharem[...] = shares

    load_moe.wait()

    def norm_rows(b, carry):
        at = pl.ds(pl.multiple_of(b * 32, 32), 32)
        f = xin[at, :].astype(F32)
        scaled = f * lax.rsqrt(jnp.mean(f * f, axis=-1, keepdims=True) + 1e-06)
        xn[at, :] = (scaled * mgain_ref[...]).astype(BF16)
        return carry

    lax.fori_loop(0, 4, norm_rows, 0)

    def pack(dst, first):
        def one(i, carry):
            dst[first + i] = scr[pl.ds(pl.multiple_of(i * PITCH, 8), BLOCK), :].astype(BF16)
            return carry

        lax.fori_loop(0, GSIZE, one, 0, unroll=4)

    def unpack(src, first):
        def one(i, carry):
            scr[pl.ds(pl.multiple_of(i * PITCH, 8), BLOCK), :] = src[first + i].astype(F32)
            return carry

        lax.fori_loop(0, GSIZE, one, 0, unroll=4)

    def spread(got, first):
        for r in range(CAP):
            for q in range(4):
                scr[pl.ds(r * PIECES + first + q, GSIZE, stride=PITCH), :] = got[
                    r * GSIZE : (r + 1) * GSIZE, q * 128 : (q + 1) * 128
                ]

    def gather(g, carry):
        ranks = rankm[pl.ds(pl.multiple_of(g * GSIZE, GSIZE), GSIZE), :]
        take = jnp.concatenate([jnp.where(ranks == float(r), 1.0, 0.0) for r in range(CAP)], axis=0).astype(BF16)
        for n in range(4):
            spread(jnp.dot(take, xn[:, n * 512 : (n + 1) * 512], preferred_element_type=F32), n * 4)
        pack(sbuf, g * GSIZE)
        return carry

    lax.fori_loop(0, GROUPS, gather, 0)
    load_value.wait()
    load_gate.wait()
    for load in load_w:
        load.wait()
    pl.semaphore_wait(barrier, PEERS - 1)

    nxt = (me + 1) & 127
    halo_copies = []
    for n, half in enumerate((value, gate)):
        cp = pltpu.make_async_remote_copy(
            src_ref=half.at[pl.ds(1024 - HALO, HALO), :], dst_ref=halo.at[n],
            send_sem=halo_send.at[n], recv_sem=halo_recv.at[n],
            device_id=(nxt >> 3, nxt & 7), device_id_type=MESH,
        )
        cp.start()
        halo_copies.append(cp)

    def w_block(n, rows_at, stage, target):
        pltpu.make_async_remote_copy(
            src_ref=wfull.at[n, rows_at, :], dst_ref=wfull.at[n, rows_at, :],
            send_sem=w_send.at[stage], recv_sem=w_recv.at[stage], device_id=target, device_id_type=MESH,
        ).start()

    def w_wait(sem, blocks):
        some = obuf.at[pl.ds(0, 16 * blocks), :]
        pltpu.make_async_copy(some, some, sem).wait()

    def origin(d):
        return pl.ds(pl.multiple_of((((y - d) & 3) * 2 + c) * 128, 128), 128)

    for d in range(1, 4):
        w_block(x, shard, 0, device(0, 0, d, 0))
        w_block(4 + z, shard, 0, device(0, 0, d, 0))
    own_forward = pltpu.make_async_remote_copy(
        src_ref=wfull.at[:, shard, :], dst_ref=wfull.at[:, shard, :], send_sem=own_send, recv_sem=own_recv,
        device_id=device(0, 0, 0, 1), device_id_type=MESH,
    )
    own_forward.start()

    self_copy = pltpu.make_async_copy(sbuf.at[0], abuf.at[0], self_sem.at[0])
    self_copy.start()

    def send_group(g):
        def send(i, carry):
            pltpu.make_async_remote_copy(
                src_ref=sbuf.at[i], dst_ref=abuf.at[i], send_sem=d_send, recv_sem=d_recv.at[g],
                device_id=device(*displacement(i)), device_id_type=MESH,
            ).start()
            return carry

        lax.fori_loop(max(1, g * GSIZE), (g + 1) * GSIZE, send, 0)

    send_group(0)
    send_group(1)

    def glu_rows(b, carry):
        at = pl.ds(pl.multiple_of(b * 32, 32), 32)
        to = pl.ds(pl.multiple_of(b * 32 + HALO, 32), 32)
        gated = value[at, :].astype(F32) * sigmoid(gate[at, :].astype(F32))
        for l in range(8):
            glu[l, to, :] = gated[:, l * 128 : (l + 1) * 128]
        return carry

    lax.fori_loop(0, 1024 // 32, glu_rows, 0)
    for cp in halo_copies:
        cp.wait()
    border = halo[0].astype(F32) * sigmoid(halo[1].astype(F32))
    border = border * jnp.minimum(me, 1).astype(F32)
    for l in range(8):
        glu[l, pl.ds(0, HALO), :] = border[:, l * 128 : (l + 1) * 128]
        glu[l, pl.ds(1024 + HALO, 8), :] = jnp.zeros((8, 128), F32)

    def conv_block(n, carry):
        l, block = n // CONV_BLOCKS, n % CONV_BLOCKS
        lanes = pl.ds(pl.multiple_of(l * 128, 128), 128)
        b0 = jnp.minimum(block * CONV_STEP, SEGMENT - CONV_STEP)
        near = [glu[l, pl.ds(b0 + 2 + u, 8, stride=SEGMENT), :] for u in range(CONV_STEP + 30)]
        totals = [None] * CONV_STEP
        for tap in range(31):
            w = jnp.broadcast_to(taps_ref[tap : tap + 1, lanes], (8, 128))
            for b in range(CONV_STEP):
                term = w * near[b + tap]
                totals[b] = term if tap == 0 else totals[b] + term
        for b in range(CONV_STEP):
            conv[l, pl.ds(b0 + b, 8, stride=SEGMENT), :] = totals[b]
        return carry

    lax.fori_loop(0, 8 * CONV_BLOCKS, conv_block, 0)

    w_wait(w_recv.at[0], 6)
    for d in range(1, 4):
        for e in range(1, 4):
            w_block(x, origin(d), 1, device(0, e, 0, 0))
            w_block(4 + z, origin(d), 1, device(e, 0, 0, 0))
    send_group(2)
    send_group(3)

    def norm_conv(n, carry):
        at = pl.ds(pl.multiple_of(n * 32, 32), 32)
        v = jnp.concatenate([conv[l, at, :] for l in range(8)], axis=-1)
        center = jnp.mean(v, axis=-1, keepdims=True)
        v = v - center
        spread = jnp.mean(v * v, axis=-1, keepdims=True)
        u = v * lax.rsqrt(spread + 1e-05) * cgain_ref[...] + cshift_ref[...]
        act[at, :] = (u * sigmoid(u)).astype(BF16)
        return carry

    lax.fori_loop(0, 32, norm_conv, 0, unroll=2)

    load_wg.wait()
    load_wu.wait()
    load_wd.wait()

    def group_wait(buf, sem, g):
        n = GSIZE - 1 if g == 0 else GSIZE
        pltpu.make_async_copy(buf.at[pl.ds(0, n)], buf.at[pl.ds(0, n)], sem.at[g]).wait()

    def experts(g):
        unpack(abuf, g * GSIZE)

        def line_up(n, carry):
            cols = pl.ds(pl.multiple_of(n * 128, 128), 128)
            for r in range(CAP):
                rows[pl.ds(r * GSIZE, GSIZE), cols] = scr[pl.ds(r * PIECES + n, GSIZE, stride=PITCH), :].astype(BF16)
            return carry

        lax.fori_loop(0, PIECES, line_up, 0)

        def up(n, carry):
            cols = pl.ds(pl.multiple_of(n * 512, 512), 512)
            pre_gate = jnp.dot(rows[...], wg[:, cols], preferred_element_type=F32)
            pre_up = jnp.dot(rows[...], wu[:, cols], preferred_element_type=F32)
            gated = jnp.minimum(pre_gate, CLAMP_LIMIT)
            lifted = jnp.clip(pre_up, -CLAMP_LIMIT, CLAMP_LIMIT) + 1.0
            hidden[:, cols] = (lifted * gated * sigmoid(GLU_SLOPE * gated)).astype(BF16)
            return carry

        lax.fori_loop(0, 2, up, 0)

        def down(n, carry):
            cols = pl.ds(pl.multiple_of(n * 512, 512), 512)
            spread(jnp.dot(hidden[...], wd[:, cols], preferred_element_type=F32), n * 4)
            return carry

        lax.fori_loop(0, 4, down, 0)
        pack(rbuf, g * GSIZE)

        def give_back(i, carry):
            dz, dx, dy, dc = displacement(i)
            pltpu.make_async_remote_copy(
                src_ref=rbuf.at[i], dst_ref=tbuf.at[i], send_sem=r_send, recv_sem=r_recv.at[g],
                device_id=device(-dz, -dx, -dy, dc), device_id_type=MESH,
            ).start()
            return carry

        lax.fori_loop(max(1, g * GSIZE), (g + 1) * GSIZE, give_back, 0)

    self_copy.wait()
    for g in range(GROUPS):
        group_wait(abuf, d_recv, g)
        experts(g)
    self_back = pltpu.make_async_copy(rbuf.at[0], tbuf.at[0], self_sem.at[1])
    self_back.start()

    for r in range(CAP):
        weights[:, r * PEERS : (r + 1) * PEERS] = jnp.where(rankm[...] == float(r), sharem[...], 0.0).T.astype(BF16)

    w_wait(w_recv.at[1], 18)
    for d in range(1, 4):
        pltpu.make_async_remote_copy(
            src_ref=wfull.at[:, origin(d), :], dst_ref=wfull.at[:, origin(d), :],
            send_sem=w_send.at[2], recv_sem=w_recv.at[2], device_id=device(0, 0, 0, 1), device_id_type=MESH,
        ).start()
    own_forward.wait()
    w_wait(w_recv.at[2], 24)

    def project(n, carry):
        cols = pl.ds(pl.multiple_of(n * 256, 256), 256)
        for m in range(2):
            at = pl.ds(m * 512, 512)
            obuf[at, cols] = jnp.dot(act[at, :], wfull[n], preferred_element_type=F32).astype(BF16)
        return carry

    lax.fori_loop(0, 8, project, 0)
    store_mixed = pltpu.make_async_copy(obuf, mixed_hbm, out_sem.at[0])
    store_mixed.start()

    self_back.wait()
    for g in range(GROUPS):
        group_wait(tbuf, r_recv, g)
        unpack(tbuf, g * GSIZE)

        def line_up_back(n, carry, g=g):
            cols = pl.ds(pl.multiple_of(n * 128, 128), 128)
            for r in range(CAP):
                result[pl.ds(r * PEERS + g * GSIZE, GSIZE), cols] = scr[
                    pl.ds(r * PIECES + n, GSIZE, stride=PITCH), :
                ].astype(BF16)
            return carry

        lax.fori_loop(0, PIECES, line_up_back, 0)

    def combine(n, carry):
        cols = pl.ds(pl.multiple_of(n * 512, 512), 512)
        mout[:, cols] = jnp.dot(weights[...], result[:, cols], preferred_element_type=F32).astype(BF16)
        return carry

    lax.fori_loop(0, 4, combine, 0)
    store_moe = pltpu.make_async_copy(mout, moe_out_hbm, out_sem.at[1])
    store_moe.start()
    sent = sbuf.at[pl.ds(0, PEERS - 1)]
    pltpu.make_async_copy(sent, sent, d_send).wait()
    pltpu.make_async_copy(sent, sent, r_send).wait()
    w_wait(w_send.at[0], 6)
    w_wait(w_send.at[1], 18)
    w_wait(w_send.at[2], 24)
    store_mixed.wait()
    store_moe.wait()


def copy_out(mixed_in, moe_in, mixed_out, moe_out, mixed, moe, sem_in, sem_out):
    pieces = []
    for n in range(8):
        at = pl.ds(n * 128, 128)
        pieces.append((mixed_in.at[at, :], mixed.at[at, :], mixed_out.at[at, :]))
    pieces.append((moe_in, moe, moe_out))
    reads = [pltpu.make_async_copy(a, b, sem_in.at[n]) for n, (a, b, _) in enumerate(pieces)]
    writes = [pltpu.make_async_copy(b, o, sem_out.at[n]) for n, (_, b, o) in enumerate(pieces)]
    for read in reads:
        read.start()
    for read, write in zip(reads, writes):
        read.wait()
        write.start()
    for write in writes:
        write.wait()


def body(
    glu_value, glu_gate, conv_taps, chan_gain, chan_shift, mix_out_weight, moe_input, moe_gain, expert_ids,
    expert_share, expert_gate_weight, expert_up_weight, expert_down_weight,
):
    hbm = pl.BlockSpec(memory_space=pl.ANY)
    dma = pltpu.SemaphoreType.DMA
    mixed, moe_output = pl.pallas_call(
        kernel,
        out_shape=(
            jax.ShapeDtypeStruct((1024, 2048), BF16),
            jax.ShapeDtypeStruct((128, 2048), BF16),
        ),
        in_specs=[hbm] * 13,
        out_specs=(hbm, hbm),
        scratch_shapes=[
            pltpu.VMEM((31, 1024), F32),
            pltpu.VMEM((1, 1024), F32),
            pltpu.VMEM((1, 1024), F32),
            pltpu.VMEM((1, 2048), F32),
            pltpu.VMEM((4, 128), jnp.int32),
            pltpu.VMEM((4, 128), F32),
            pltpu.VMEM((1024, 1024), BF16),
            pltpu.VMEM((1024, 1024), BF16),
            pltpu.VMEM((2, HALO, 1024), BF16),
            pltpu.VMEM((8, 1024 + HALO + 8, 128), F32),
            pltpu.VMEM((8, 8 * SEGMENT, 128), F32),
            pltpu.VMEM((1024, 1024), BF16),
            pltpu.VMEM((8, 1024, 256), BF16),
            pltpu.VMEM((1024, 2048), BF16),
            pltpu.VMEM((128, 2048), BF16),
            pltpu.VMEM((128, 2048), BF16),
            pltpu.VMEM((128, PEERS), F32),
            pltpu.VMEM((128, PEERS), F32),
            pltpu.VMEM((PEERS, BLOCK, 128), BF16),
            pltpu.VMEM((PEERS, BLOCK, 128), BF16),
            pltpu.VMEM((PEERS, BLOCK, 128), BF16),
            pltpu.VMEM((PEERS, BLOCK, 128), BF16),
            pltpu.VMEM((GSIZE * PITCH, 128), F32),
            pltpu.VMEM((GSIZE * CAP, 2048), BF16),
            pltpu.VMEM((GSIZE * CAP, 1024), BF16),
            pltpu.VMEM((2048, 1024), BF16),
            pltpu.VMEM((2048, 1024), BF16),
            pltpu.VMEM((1024, 2048), BF16),
            pltpu.VMEM((PEERS * CAP, 2048), BF16),
            pltpu.VMEM((128, CAP * PEERS), BF16),
            pltpu.VMEM((128, 2048), BF16),
            dma((21,)), dma((2,)), dma((2,)), dma((2,)), dma((3,)), dma((3,)), dma, dma,
            dma, dma((GROUPS,)), dma, dma((GROUPS,)), dma((2,)),
        ],
        compiler_params=pltpu.CompilerParams(
            collective_id=0, has_side_effects=True, vmem_limit_bytes=62 * 2**20
        ),
        name="mixer",
    )(
        glu_value, glu_gate, conv_taps, chan_gain.reshape(1, -1), chan_shift.reshape(1, -1), mix_out_weight,
        moe_input, moe_gain.reshape(1, -1), expert_ids.T, expert_share.T,
        expert_gate_weight, expert_up_weight, expert_down_weight,
    )
    shapes = (mixed.shape, moe_output.shape)
    return pl.pallas_call(
        copy_out,
        out_shape=tuple(jax.ShapeDtypeStruct(shape, BF16) for shape in shapes),
        in_specs=[pl.BlockSpec(memory_space=pltpu.HBM)] * 2,
        out_specs=(pl.BlockSpec(memory_space=pltpu.HBM),) * 2,
        scratch_shapes=[*(pltpu.VMEM(shape, BF16) for shape in shapes), dma((9,)), dma((9,))],
        compiler_params=pltpu.CompilerParams(vmem_limit_bytes=63 * 2**20),
        name="copy_out",
    )(mixed, moe_output)


def solution(mesh):
    both = ("ep", "tp")
    placed = (
        P(both, None), P(both, None), P(), P(), P(), P("tp", None), P(both, None), P(), P(both, None),
        P(both, None), P(both, None, None), P(both, None, None), P(both, None, None),
    )
    return jax.shard_map(
        body,
        mesh=mesh,
        in_specs=placed,
        out_specs=(P(both, None), P(both, None)),
        check_vma=False,
    )
```

time: 115 us -> 99.7 us (0.87)
  local copies, waits for them, and re-layouts: 8.47 us -> 0 us
  Pallas kernels: 105 us -> 98.9 us
    pallas_call x1, Pallas kernels: 105 us -> 94.8 us  [body(): pl.pallas_call(kernel, out_shape=(jax.ShapeDtypeStruct((1024, 2048), BF16...]
    unnamed x6 -> x0, local copies, waits for them, and re-layouts: 8.47 us -> none
    pallas_call x0 -> x1, Pallas kernels: none -> 4.16 us  [body(): pl.pallas_call(copy_out, out_shape=tuple((jax.ShapeDtypeStruct(shape, BF1...]
where the time goes in v2:
time: 99.7 us; the launch traced here: 99.6 us
  Pallas kernels  98.9 us (99%)
    pallas_call x1, Pallas kernels, body(): pl.pallas_call(kernel, out_shape=(jax.ShapeDtypeStruct((1024, 2048), BF16...  94.8 us
    pallas_call x1, Pallas kernels, body(): pl.pallas_call(copy_out, out_shape=tuple((jax.ShapeDtypeStruct(shape, BF1...  4.16 us

profile of v2, /device:TPU:1, one launch (start us, length us, event | category | flops | bytes accessed | tf_op | source)
XLA Modules:
  0.0 99.6 jit_solution(18141628208488428458)
XLA Ops:
  0.6 94.8 %mixer.1 = (bf16[1024,2048]{1,0:T(8,128)(2,1)}, bf16[128,2048]{1,0:T(8,128)(2,1)}) custom-call(bf16[1024,1024]{1,0:T(8,128)(2,1)} %value_hbm.1, bf16[1024,1024]{1,0:T(8,128)(2,1)} %gate_hbm.1, f32[31,1024]{1,0:T(8,128)} %taps_hbm.1, f32[1,1024]{1,0:T(1,128)} %bitcast.6, f32[1,1024]{1,0:T(1,128)} %bitcast.7, bf16[128,2048]{1,0:T(8,128)(2,1)} %wout_hbm.1, ...), custom_call_target="tpu_custom_call" | custom-call | tf_op jit(solution)/shard_map/mixer/pallas_call | solution.py:386
  95.4 4.2 %copy_out.1 = (bf16[1024,2048]{1,0:T(8,128)(2,1)}, bf16[128,2048]{1,0:T(8,128)(2,1)}) custom-call(bf16[1024,2048]{1,0:T(8,128)(2,1)} %get-tuple-element.4.mixed_in, bf16[128,2048]{1,0:T(8,128)(2,1)} %get-tuple-element.5.moe_in), custom_call_target="tpu_custom_call" | custom-call | tf_op jit(solution)/shard_map/copy_out/pallas_call | solution.py:439

commit v3 on v2

--- a/solution.py
+++ b/solution.py
@@ -1,7 +1,6 @@
-import functools
-
 import jax
 import jax.numpy as jnp
+import numpy as np
 from jax import lax
 from jax.experimental import pallas as pl
 from jax.experimental.pallas import tpu as pltpu
@@ -14,7 +13,6 @@
 GLU_SLOPE = 1.702
 CAP = 5
 PEERS = 128
-SCRAMBLE = 101
 GROUPS = 4
 GSIZE = PEERS // GROUPS
 PIECES = 16
@@ -23,6 +21,8 @@
 HALO = 32
 SEGMENT = 129
 CONV_STEP = 12
+EARLY = 3
+BORDER = 3
 CONV_BLOCKS = -(-SEGMENT // CONV_STEP)
 
 
@@ -30,17 +30,54 @@
     return 0.5 + 0.5 * jnp.tanh(0.5 * v)
 
 
-def displacement(i):
-    j = (i * SCRAMBLE) & (PEERS - 1)
-    return j >> 5, j >> 3, j >> 1, j
+CLASSES = (
+    ("220", "210", "120", "110", "200", "020", "100", "010", "000"),
+    ("222", "212", "122", "221", "211", "121", "202"),
+    ("022", "112", "111", "102", "002"),
+    ("012", "201", "021", "101", "011", "001"),
+)
+SELF = 31
+
+
+def steps(pattern, k):
+    out, bit = [], 1
+    for axis in pattern:
+        if axis == "1":
+            out.append(1 + 2 * ((k >> bit) & 1))
+            bit += 1
+        else:
+            out.append(int(axis))
+    return (*out, 1 - (k & 1))
+
+
+def loops():
+    groups, first = [], 0
+    for patterns in CLASSES:
+        groups.append([])
+        for pattern in patterns:
+            count = 2 << pattern.count("1")
+            groups[-1].append((first, count, pattern))
+            first += count
+        assert first == GSIZE * len(groups)
+    return groups
+
+
+def places():
+    flat = []
+    for first, count, pattern in sum(loops(), []):
+        for k in range(count):
+            dz, dx, dy, dc = steps(pattern, k)
+            flat.append(dz * 32 + dx * 8 + dy * 2 + dc)
+    assert sorted(flat) == list(range(PEERS)) and flat[SELF] == 0
+    return np.repeat(np.array(flat, np.int32)[:, None], 128, axis=1)
 
 
 def kernel(
-    value_hbm, gate_hbm, taps_hbm, cgain_hbm, cshift_hbm, wout_hbm, moe_hbm, mgain_hbm, ids_hbm, share_hbm,
+    value_hbm, gate_hbm, taps_hbm, cgain_hbm, cshift_hbm, wout_hbm, moe_hbm, mgain_hbm, ids_hbm, share_hbm, place_hbm,
     wg_hbm, wu_hbm, wd_hbm,
     mixed_hbm, moe_out_hbm,
-    taps_ref, cgain_ref, cshift_ref, mgain_ref, ids_ref, share_ref, value, gate, halo, glu, conv, act, wfull, obuf,
-    xin, xn, rankm, sharem, sbuf, abuf, rbuf, tbuf, scr, rows, hidden, wg, wu, wd, result, weights, mout,
+    taps_ref, cgain_ref, cshift_ref, mgain_ref, ids_ref, share_ref, place_ref, value, gate, halo, glu, conv, act, wfull, obuf,
+    xin, xn, rankm, sharem, sbuf, abuf, rbuf, tbuf, scr, rows, hidden, wg, wu, wd, result, weights, acc, mout,
     local_sem, out_sem, halo_send, halo_recv, w_send, w_recv, own_send, own_recv,
     d_send, d_recv, r_send, r_recv, self_sem,
 ):
@@ -52,17 +89,9 @@
     def device(dz, dx, dy, dc):
         return ((z + dz) & 3) * 4 + ((x + dx) & 3), ((y + dy) & 3) * 2 + ((c + dc) & 1)
 
-    barrier = pltpu.get_barrier_semaphore()
-
-    def hello(i, carry):
-        pl.semaphore_signal(barrier, inc=1, device_id=device(*displacement(i)), device_id_type=MESH)
-        return carry
-
-    lax.fori_loop(1, PEERS, hello, 0, unroll=3)
-
     shard = pl.ds(pl.multiple_of(tp * 128, 128), 128)
     pairs = (
-        (ids_hbm, ids_ref), (share_hbm, share_ref), (mgain_hbm, mgain_ref),
+        (ids_hbm, ids_ref), (share_hbm, share_ref), (place_hbm, place_ref), (mgain_hbm, mgain_ref),
         (taps_hbm, taps_ref), (cgain_hbm, cgain_ref), (cshift_hbm, cshift_ref),
     )
     small = [pltpu.make_async_copy(a, b, local_sem.at[15 + n]) for n, (a, b) in enumerate(pairs)]
@@ -76,15 +105,27 @@
     load_wg = pltpu.make_async_copy(wg_hbm.at[0], wg, local_sem.at[4])
     load_wu = pltpu.make_async_copy(wu_hbm.at[0], wu, local_sem.at[5])
     load_wd = pltpu.make_async_copy(wd_hbm.at[0], wd, local_sem.at[6])
-    for load in (*small, load_moe, *load_w, load_value, load_gate, load_wg, load_wu, load_wd):
+    for load in (*small[:4], load_moe):
         load.start()
 
-    for load in small:
+    barrier = pltpu.get_barrier_semaphore()
+
+    def hello(i, carry):
+        target = me ^ i
+        pl.semaphore_signal(barrier, inc=1, device_id=(target >> 3, target & 7), device_id_type=MESH)
+        return carry
+
+    lax.fori_loop(1, PEERS, hello, 0, unroll=3)
+
+    for load in (*load_w, load_value, load_gate, *small[4:], load_wg, load_wu, load_wd):
+        load.start()
+
+    for load in small[:4]:
         load.wait()
 
     lane = lax.broadcasted_iota(jnp.int32, (PEERS, 128), 1)
     row = lax.broadcasted_iota(jnp.int32, (PEERS, 128), 0)
-    j = (row * SCRAMBLE) & 127
+    j = place_ref[...]
     expert = (
         (((z + (j >> 5)) & 3) * 32) + (((x + (j >> 3)) & 3) * 8) + (((y + (j >> 1)) & 3) * 2) + ((c + j) & 1)
     )
@@ -164,7 +205,7 @@
         ).start()
 
     def w_wait(sem, blocks):
-        some = obuf.at[pl.ds(0, 16 * blocks), :]
+        some = act.at[pl.ds(0, 32 * blocks), :]
         pltpu.make_async_copy(some, some, sem).wait()
 
     def origin(d):
@@ -179,21 +220,30 @@
     )
     own_forward.start()
 
-    self_copy = pltpu.make_async_copy(sbuf.at[0], abuf.at[0], self_sem.at[0])
+    self_copy = pltpu.make_async_copy(sbuf.at[SELF], abuf.at[SELF], self_sem.at[0])
     self_copy.start()
 
+    sends = loops()
+
+    def each(g, act_on):
+        for first, count, pattern in sends[g]:
+
+            def one(k, carry, first=first, pattern=pattern):
+                act_on(first + k, steps(pattern, k))
+                return carry
+
+            lax.fori_loop(0, count - (pattern == "000"), one, 0)
+
     def send_group(g):
-        def send(i, carry):
+        def send(i, d):
             pltpu.make_async_remote_copy(
                 src_ref=sbuf.at[i], dst_ref=abuf.at[i], send_sem=d_send, recv_sem=d_recv.at[g],
-                device_id=device(*displacement(i)), device_id_type=MESH,
+                device_id=device(*d), device_id_type=MESH,
             ).start()
-            return carry
-
-        lax.fori_loop(max(1, g * GSIZE), (g + 1) * GSIZE, send, 0)
+
+        each(g, send)
 
     send_group(0)
-    send_group(1)
 
     def glu_rows(b, carry):
         at = pl.ds(pl.multiple_of(b * 32, 32), 32)
@@ -204,16 +254,12 @@
         return carry
 
     lax.fori_loop(0, 1024 // 32, glu_rows, 0)
-    for cp in halo_copies:
-        cp.wait()
-    border = halo[0].astype(F32) * sigmoid(halo[1].astype(F32))
-    border = border * jnp.minimum(me, 1).astype(F32)
+    for g in range(1, GROUPS):
+        send_group(g)
     for l in range(8):
-        glu[l, pl.ds(0, HALO), :] = border[:, l * 128 : (l + 1) * 128]
         glu[l, pl.ds(1024 + HALO, 8), :] = jnp.zeros((8, 128), F32)
 
-    def conv_block(n, carry):
-        l, block = n // CONV_BLOCKS, n % CONV_BLOCKS
+    def conv_block(l, block):
         lanes = pl.ds(pl.multiple_of(l * 128, 128), 128)
         b0 = jnp.minimum(block * CONV_STEP, SEGMENT - CONV_STEP)
         near = [glu[l, pl.ds(b0 + 2 + u, 8, stride=SEGMENT), :] for u in range(CONV_STEP + 30)]
@@ -225,17 +271,26 @@
                 totals[b] = term if tap == 0 else totals[b] + term
         for b in range(CONV_STEP):
             conv[l, pl.ds(b0 + b, 8, stride=SEGMENT), :] = totals[b]
-        return carry
-
-    lax.fori_loop(0, 8 * CONV_BLOCKS, conv_block, 0)
-
-    w_wait(w_recv.at[0], 6)
-    for d in range(1, 4):
-        for e in range(1, 4):
-            w_block(x, origin(d), 1, device(0, e, 0, 0))
-            w_block(4 + z, origin(d), 1, device(e, 0, 0, 0))
-    send_group(2)
-    send_group(3)
+
+    def conv_blocks(first, last):
+        def one(n, carry):
+            conv_block(n & 7, first + (n >> 3))
+            return carry
+
+        lax.fori_loop(0, 8 * (last - first), one, 0)
+
+    for load in small[4:]:
+        load.wait()
+    conv_blocks(BORDER, BORDER + EARLY)
+
+    for cp in halo_copies:
+        cp.wait()
+    border = halo[0].astype(F32) * sigmoid(halo[1].astype(F32))
+    border = border * jnp.minimum(me, 1).astype(F32)
+    for l in range(8):
+        glu[l, pl.ds(0, HALO), :] = border[:, l * 128 : (l + 1) * 128]
+    conv_blocks(0, BORDER)
+    conv_blocks(BORDER + EARLY, CONV_BLOCKS)
 
     def norm_conv(n, carry):
         at = pl.ds(pl.multiple_of(n * 32, 32), 32)
@@ -287,25 +342,36 @@
         lax.fori_loop(0, 4, down, 0)
         pack(rbuf, g * GSIZE)
 
-        def give_back(i, carry):
-            dz, dx, dy, dc = displacement(i)
+        def give_back(i, d):
+            dz, dx, dy, dc = d
             pltpu.make_async_remote_copy(
                 src_ref=rbuf.at[i], dst_ref=tbuf.at[i], send_sem=r_send, recv_sem=r_recv.at[g],
                 device_id=device(-dz, -dx, -dy, dc), device_id_type=MESH,
             ).start()
-            return carry
-
-        lax.fori_loop(max(1, g * GSIZE), (g + 1) * GSIZE, give_back, 0)
+
+        each(g, give_back)
+
+    w_wait(w_recv.at[0], 6)
+    for d in range(1, 4):
+        for e in range(1, 4):
+            w_block(x, origin(d), 1, device(0, e, 0, 0))
+            w_block(4 + z, origin(d), 1, device(e, 0, 0, 0))
 
     self_copy.wait()
-    for g in range(GROUPS):
+    group_wait(abuf, d_recv, 0)
+    experts(0)
+    self_back = pltpu.make_async_copy(rbuf.at[SELF], tbuf.at[SELF], self_sem.at[1])
+    self_back.start()
+
+    for g in range(1, GROUPS):
         group_wait(abuf, d_recv, g)
         experts(g)
-    self_back = pltpu.make_async_copy(rbuf.at[0], tbuf.at[0], self_sem.at[1])
-    self_back.start()
-
-    for r in range(CAP):
-        weights[:, r * PEERS : (r + 1) * PEERS] = jnp.where(rankm[...] == float(r), sharem[...], 0.0).T.astype(BF16)
+
+    for g in range(GROUPS):
+        ranks = rankm[g * GSIZE : (g + 1) * GSIZE, :]
+        parts = sharem[g * GSIZE : (g + 1) * GSIZE, :]
+        stacked = jnp.concatenate([jnp.where(ranks == float(r), parts, 0.0) for r in range(CAP)], axis=0)
+        weights[pl.ds(g * GSIZE * CAP, GSIZE * CAP), :] = stacked.astype(BF16)
 
     w_wait(w_recv.at[1], 18)
     for d in range(1, 4):
@@ -324,10 +390,19 @@
         return carry
 
     lax.fori_loop(0, 8, project, 0)
+
     store_mixed = pltpu.make_async_copy(obuf, mixed_hbm, out_sem.at[0])
     store_mixed.start()
 
     self_back.wait()
+
+    def combine(first, n, last):
+        at = pl.ds(first * GSIZE * CAP, (last - first) * GSIZE * CAP)
+        cols = pl.ds(pl.multiple_of(n * 512, 512), 512)
+        return lax.dot_general(
+            weights[at, :], result[at, cols], (((0,), (0,)), ((), ())), preferred_element_type=F32
+        ), cols
+
     for g in range(GROUPS):
         group_wait(tbuf, r_recv, g)
         unpack(tbuf, g * GSIZE)
@@ -335,19 +410,19 @@
         def line_up_back(n, carry, g=g):
             cols = pl.ds(pl.multiple_of(n * 128, 128), 128)
             for r in range(CAP):
-                result[pl.ds(r * PEERS + g * GSIZE, GSIZE), cols] = scr[
+                result[pl.ds((g * CAP + r) * GSIZE, GSIZE), cols] = scr[
                     pl.ds(r * PIECES + n, GSIZE, stride=PITCH), :
                 ].astype(BF16)
             return carry
 
         lax.fori_loop(0, PIECES, line_up_back, 0)
-
-    def combine(n, carry):
-        cols = pl.ds(pl.multiple_of(n * 512, 512), 512)
-        mout[:, cols] = jnp.dot(weights[...], result[:, cols], preferred_element_type=F32).astype(BF16)
-        return carry
-
-    lax.fori_loop(0, 4, combine, 0)
+        if g == GROUPS - 2:
+            for n in range(4):
+                got, cols = combine(0, n, GROUPS - 1)
+                acc[:, cols] = got
+    for n in range(4):
+        got, cols = combine(GROUPS - 1, n, GROUPS)
+        mout[:, cols] = (acc[:, cols] + got).astype(BF16)
     store_moe = pltpu.make_async_copy(mout, moe_out_hbm, out_sem.at[1])
     store_moe.start()
     sent = sbuf.at[pl.ds(0, PEERS - 1)]
@@ -389,7 +464,7 @@
             jax.ShapeDtypeStruct((1024, 2048), BF16),
             jax.ShapeDtypeStruct((128, 2048), BF16),
         ),
-        in_specs=[hbm] * 13,
+        in_specs=[hbm] * 14,
         out_specs=(hbm, hbm),
         scratch_shapes=[
             pltpu.VMEM((31, 1024), F32),
@@ -398,6 +473,7 @@
             pltpu.VMEM((1, 2048), F32),
             pltpu.VMEM((4, 128), jnp.int32),
             pltpu.VMEM((4, 128), F32),
+            pltpu.VMEM((PEERS, 128), jnp.int32),
             pltpu.VMEM((1024, 1024), BF16),
             pltpu.VMEM((1024, 1024), BF16),
             pltpu.VMEM((2, HALO, 1024), BF16),
@@ -421,9 +497,10 @@
             pltpu.VMEM((2048, 1024), BF16),
             pltpu.VMEM((1024, 2048), BF16),
             pltpu.VMEM((PEERS * CAP, 2048), BF16),
-            pltpu.VMEM((128, CAP * PEERS), BF16),
+            pltpu.VMEM((CAP * PEERS, 128), BF16),
+            pltpu.VMEM((128, 2048), F32),
             pltpu.VMEM((128, 2048), BF16),
-            dma((21,)), dma((2,)), dma((2,)), dma((2,)), dma((3,)), dma((3,)), dma, dma,
+            dma((22,)), dma((2,)),  dma((2,)), dma((2,)), dma((3,)), dma((3,)), dma, dma,
             dma, dma((GROUPS,)), dma, dma((GROUPS,)), dma((2,)),
         ],
         compiler_params=pltpu.CompilerParams(
@@ -432,15 +509,15 @@
         name="mixer",
     )(
         glu_value, glu_gate, conv_taps, chan_gain.reshape(1, -1), chan_shift.reshape(1, -1), mix_out_weight,
-        moe_input, moe_gain.reshape(1, -1), expert_ids.T, expert_share.T,
+        moe_input, moe_gain.reshape(1, -1), expert_ids.T, expert_share.T, places(),
         expert_gate_weight, expert_up_weight, expert_down_weight,
     )
     shapes = (mixed.shape, moe_output.shape)
     return pl.pallas_call(
         copy_out,
         out_shape=tuple(jax.ShapeDtypeStruct(shape, BF16) for shape in shapes),
-        in_specs=[pl.BlockSpec(memory_space=pltpu.HBM)] * 2,
-        out_specs=(pl.BlockSpec(memory_space=pltpu.HBM),) * 2,
+        in_specs=[hbm, hbm],
+        out_specs=(hbm, hbm),
         scratch_shapes=[*(pltpu.VMEM(shape, BF16) for shape in shapes), dma((9,)), dma((9,))],
         compiler_params=pltpu.CompilerParams(vmem_limit_bytes=63 * 2**20),
         name="copy_out",

time: 99.7 us -> 94.1 us (0.944)
  Pallas kernels: 98.9 us -> 93.3 us
    pallas_call x1, Pallas kernels: 94.8 us -> 89.2 us  [body(): pl.pallas_call(kernel, out_shape=(jax.ShapeDtypeStruct((1024, 2048), BF16...]
where the time goes in v3:
time: 94.1 us; the launch traced here: 94 us
  Pallas kernels  93.3 us (99%)
    pallas_call x1, Pallas kernels, body(): pl.pallas_call(kernel, out_shape=(jax.ShapeDtypeStruct((1024, 2048), BF16...  89.2 us
    pallas_call x1, Pallas kernels, body(): pl.pallas_call(copy_out, out_shape=tuple((jax.ShapeDtypeStruct(shape, BF1...  4.16 us

profile of v3, /device:TPU:1, one launch (start us, length us, event | category | flops | bytes accessed | tf_op | source)
XLA Modules:
  0.0 94.0 jit_solution(15492196371235007593)
XLA Ops:
  0.6 89.2 %mixer.1 = (bf16[1024,2048]{1,0:T(8,128)(2,1)}, bf16[128,2048]{1,0:T(8,128)(2,1)}) custom-call(bf16[1024,1024]{1,0:T(8,128)(2,1)} %value_hbm.1, bf16[1024,1024]{1,0:T(8,128)(2,1)} %gate_hbm.1, f32[31,1024]{1,0:T(8,128)} %taps_hbm.1, f32[1,1024]{1,0:T(1,128)} %bitcast.6, f32[1,1024]{1,0:T(1,128)} %bitcast.7, bf16[128,2048]{1,0:T(8,128)(2,1)} %wout_hbm.1, ...), custom_call_target="tpu_custom_call" | custom-call | tf_op jit(solution)/shard_map/mixer/pallas_call | solution.py:461
  89.8 4.2 %copy_out.1 = (bf16[1024,2048]{1,0:T(8,128)(2,1)}, bf16[128,2048]{1,0:T(8,128)(2,1)}) custom-call(bf16[1024,2048]{1,0:T(8,128)(2,1)} %get-tuple-element.4.mixed_in, bf16[128,2048]{1,0:T(8,128)(2,1)} %get-tuple-element.5.moe_in), custom_call_target="tpu_custom_call" | custom-call | tf_op jit(solution)/shard_map/copy_out/pallas_call | solution.py:516

commit v4 on v3

--- a/solution.py
+++ b/solution.py
@@ -76,7 +76,7 @@
     value_hbm, gate_hbm, taps_hbm, cgain_hbm, cshift_hbm, wout_hbm, moe_hbm, mgain_hbm, ids_hbm, share_hbm, place_hbm,
     wg_hbm, wu_hbm, wd_hbm,
     mixed_hbm, moe_out_hbm,
-    taps_ref, cgain_ref, cshift_ref, mgain_ref, ids_ref, share_ref, place_ref, value, gate, halo, glu, conv, act, wfull, obuf,
+    taps_ref, cgain_ref, cshift_ref, mgain_ref, ids_ref, share_ref, place_ref, value, gate, edge, halo, glu, conv, act, wfull, obuf,
     xin, xn, rankm, sharem, sbuf, abuf, rbuf, tbuf, scr, rows, hidden, wg, wu, wd, result, weights, acc, mout,
     local_sem, out_sem, halo_send, halo_recv, w_send, w_recv, own_send, own_recv,
     d_send, d_recv, r_send, r_recv, self_sem,
@@ -105,19 +105,24 @@
     load_wg = pltpu.make_async_copy(wg_hbm.at[0], wg, local_sem.at[4])
     load_wu = pltpu.make_async_copy(wu_hbm.at[0], wu, local_sem.at[5])
     load_wd = pltpu.make_async_copy(wd_hbm.at[0], wd, local_sem.at[6])
-    for load in (*small[:4], load_moe):
+    ends = pl.ds(1024 - HALO, HALO)
+    load_ends = [
+        pltpu.make_async_copy(half.at[ends, :], edge.at[n], local_sem.at[22 + n])
+        for n, half in enumerate((value_hbm, gate_hbm))
+    ]
+    for load in (*small[:4], load_moe, *load_ends, *load_w):
         load.start()
 
     barrier = pltpu.get_barrier_semaphore()
 
     def hello(i, carry):
-        target = me ^ i
+        target = me ^ (PEERS - 1 - i)
         pl.semaphore_signal(barrier, inc=1, device_id=(target >> 3, target & 7), device_id_type=MESH)
         return carry
 
-    lax.fori_loop(1, PEERS, hello, 0, unroll=3)
-
-    for load in (*load_w, load_value, load_gate, *small[4:], load_wg, load_wu, load_wd):
+    lax.fori_loop(0, PEERS - 1, hello, 0, unroll=3)
+
+    for load in (load_value, load_gate, *small[4:], load_wg, load_wu, load_wd):
         load.start()
 
     for load in small[:4]:
@@ -180,18 +185,16 @@
         pack(sbuf, g * GSIZE)
         return carry
 
-    lax.fori_loop(0, GROUPS, gather, 0)
-    load_value.wait()
-    load_gate.wait()
-    for load in load_w:
+    gather(0, 0)
+    for load in (*load_ends, *load_w):
         load.wait()
     pl.semaphore_wait(barrier, PEERS - 1)
 
     nxt = (me + 1) & 127
     halo_copies = []
-    for n, half in enumerate((value, gate)):
+    for n in range(2):
         cp = pltpu.make_async_remote_copy(
-            src_ref=half.at[pl.ds(1024 - HALO, HALO), :], dst_ref=halo.at[n],
+            src_ref=edge.at[n], dst_ref=halo.at[n],
             send_sem=halo_send.at[n], recv_sem=halo_recv.at[n],
             device_id=(nxt >> 3, nxt & 7), device_id_type=MESH,
         )
@@ -244,6 +247,12 @@
         each(g, send)
 
     send_group(0)
+    lax.fori_loop(1, GROUPS, gather, 0)
+    for g in range(1, GROUPS):
+        send_group(g)
+
+    load_value.wait()
+    load_gate.wait()
 
     def glu_rows(b, carry):
         at = pl.ds(pl.multiple_of(b * 32, 32), 32)
@@ -254,8 +263,6 @@
         return carry
 
     lax.fori_loop(0, 1024 // 32, glu_rows, 0)
-    for g in range(1, GROUPS):
-        send_group(g)
     for l in range(8):
         glu[l, pl.ds(1024 + HALO, 8), :] = jnp.zeros((8, 128), F32)
 
@@ -437,8 +444,8 @@
 
 def copy_out(mixed_in, moe_in, mixed_out, moe_out, mixed, moe, sem_in, sem_out):
     pieces = []
-    for n in range(8):
-        at = pl.ds(n * 128, 128)
+    for n in range(4):
+        at = pl.ds(n * 256, 256)
         pieces.append((mixed_in.at[at, :], mixed.at[at, :], mixed_out.at[at, :]))
     pieces.append((moe_in, moe, moe_out))
     reads = [pltpu.make_async_copy(a, b, sem_in.at[n]) for n, (a, b, _) in enumerate(pieces)]
@@ -477,6 +484,7 @@
             pltpu.VMEM((1024, 1024), BF16),
             pltpu.VMEM((1024, 1024), BF16),
             pltpu.VMEM((2, HALO, 1024), BF16),
+            pltpu.VMEM((2, HALO, 1024), BF16),
             pltpu.VMEM((8, 1024 + HALO + 8, 128), F32),
             pltpu.VMEM((8, 8 * SEGMENT, 128), F32),
             pltpu.VMEM((1024, 1024), BF16),
@@ -500,7 +508,7 @@
             pltpu.VMEM((CAP * PEERS, 128), BF16),
             pltpu.VMEM((128, 2048), F32),
             pltpu.VMEM((128, 2048), BF16),
-            dma((22,)), dma((2,)),  dma((2,)), dma((2,)), dma((3,)), dma((3,)), dma, dma,
+            dma((24,)), dma((2,)),  dma((2,)), dma((2,)), dma((3,)), dma((3,)), dma, dma,
             dma, dma((GROUPS,)), dma, dma((GROUPS,)), dma((2,)),
         ],
         compiler_params=pltpu.CompilerParams(
@@ -518,7 +526,7 @@
         out_shape=tuple(jax.ShapeDtypeStruct(shape, BF16) for shape in shapes),
         in_specs=[hbm, hbm],
         out_specs=(hbm, hbm),
-        scratch_shapes=[*(pltpu.VMEM(shape, BF16) for shape in shapes), dma((9,)), dma((9,))],
+        scratch_shapes=[*(pltpu.VMEM(shape, BF16) for shape in shapes), dma((5,)), dma((5,))],
         compiler_params=pltpu.CompilerParams(vmem_limit_bytes=63 * 2**20),
         name="copy_out",
     )(mixed, moe_output)

time: 94.1 us -> 92.6 us (0.984)
  Pallas kernels: 93.3 us -> 91.8 us
    pallas_call x1, Pallas kernels: 89.2 us -> 88.2 us  [body(): pl.pallas_call(kernel, out_shape=(jax.ShapeDtypeStruct((1024, 2048), BF16...]
where the time goes in v4:
time: 92.6 us; the launch traced here: 92.4 us
  Pallas kernels  91.8 us (99%)
    pallas_call x1, Pallas kernels, body(): pl.pallas_call(kernel, out_shape=(jax.ShapeDtypeStruct((1024, 2048), BF16...  88.2 us
    pallas_call x1, Pallas kernels, body(): pl.pallas_call(copy_out, out_shape=tuple((jax.ShapeDtypeStruct(shape, BF1...  3.63 us

profile of v4, /device:TPU:1, one launch (start us, length us, event | category | flops | bytes accessed | tf_op | source)
XLA Modules:
  0.0 92.4 jit_solution(12281201117840400303)
XLA Ops:
  0.6 88.2 %mixer.1 = (bf16[1024,2048]{1,0:T(8,128)(2,1)}, bf16[128,2048]{1,0:T(8,128)(2,1)}) custom-call(bf16[1024,1024]{1,0:T(8,128)(2,1)} %value_hbm.1, bf16[1024,1024]{1,0:T(8,128)(2,1)} %gate_hbm.1, f32[31,1024]{1,0:T(8,128)} %taps_hbm.1, f32[1,1024]{1,0:T(1,128)} %bitcast.6, f32[1,1024]{1,0:T(1,128)} %bitcast.7, bf16[128,2048]{1,0:T(8,128)(2,1)} %wout_hbm.1, ...), custom_call_target="tpu_custom_call" | custom-call | tf_op jit(solution)/shard_map/mixer/pallas_call | solution.py:468
  88.8 3.6 %copy_out.1 = (bf16[1024,2048]{1,0:T(8,128)(2,1)}, bf16[128,2048]{1,0:T(8,128)(2,1)}) custom-call(bf16[1024,2048]{1,0:T(8,128)(2,1)} %get-tuple-element.4.mixed_in, bf16[128,2048]{1,0:T(8,128)(2,1)} %get-tuple-element.5.moe_in), custom_call_target="tpu_custom_call" | custom-call | tf_op jit(solution)/shard_map/copy_out/pallas_call | solution.py:524

commit v5 on v4

--- a/solution.py
+++ b/solution.py
@@ -37,6 +37,11 @@
     ("012", "201", "021", "101", "011", "001"),
 )
 SELF = 31
+LAST = (PEERS - GSIZE) * CAP
+
+
+def weighted(weights, rows):
+    return lax.dot_general(weights, rows, (((0,), (0,)), ((), ())), preferred_element_type=F32)
 
 
 def steps(pattern, k):
@@ -75,9 +80,9 @@
 def kernel(
     value_hbm, gate_hbm, taps_hbm, cgain_hbm, cshift_hbm, wout_hbm, moe_hbm, mgain_hbm, ids_hbm, share_hbm, place_hbm,
     wg_hbm, wu_hbm, wd_hbm,
-    mixed_hbm, moe_out_hbm,
+    mixed_hbm, acc_hbm, last_weights_hbm, last_hbm,
     taps_ref, cgain_ref, cshift_ref, mgain_ref, ids_ref, share_ref, place_ref, value, gate, edge, halo, glu, conv, act, wfull, obuf,
-    xin, xn, rankm, sharem, sbuf, abuf, rbuf, tbuf, scr, rows, hidden, wg, wu, wd, result, weights, acc, mout,
+    xin, xn, rankm, sharem, sbuf, abuf, rbuf, tbuf, scr, rows, hidden, wg, wu, wd, result, weights, acc,
     local_sem, out_sem, halo_send, halo_recv, w_send, w_recv, own_send, own_recv,
     d_send, d_recv, r_send, r_recv, self_sem,
 ):
@@ -351,8 +356,9 @@
 
         def give_back(i, d):
             dz, dx, dy, dc = d
+            back = last_hbm.at[i - (PEERS - GSIZE)] if g == GROUPS - 1 else tbuf.at[i]
             pltpu.make_async_remote_copy(
-                src_ref=rbuf.at[i], dst_ref=tbuf.at[i], send_sem=r_send, recv_sem=r_recv.at[g],
+                src_ref=rbuf.at[i], dst_ref=back, send_sem=r_send, recv_sem=r_recv.at[g],
                 device_id=device(-dz, -dx, -dy, dc), device_id_type=MESH,
             ).start()
 
@@ -410,7 +416,7 @@
             weights[at, :], result[at, cols], (((0,), (0,)), ((), ())), preferred_element_type=F32
         ), cols
 
-    for g in range(GROUPS):
+    for g in range(GROUPS - 1):
         group_wait(tbuf, r_recv, g)
         unpack(tbuf, g * GSIZE)
 
@@ -423,39 +429,64 @@
             return carry
 
         lax.fori_loop(0, PIECES, line_up_back, 0)
-        if g == GROUPS - 2:
-            for n in range(4):
-                got, cols = combine(0, n, GROUPS - 1)
-                acc[:, cols] = got
     for n in range(4):
-        got, cols = combine(GROUPS - 1, n, GROUPS)
-        mout[:, cols] = (acc[:, cols] + got).astype(BF16)
-    store_moe = pltpu.make_async_copy(mout, moe_out_hbm, out_sem.at[1])
-    store_moe.start()
+        cols = pl.ds(n * 512, 512)
+        acc[:, cols] = weighted(weights[pl.ds(0, LAST), :], result[pl.ds(0, LAST), cols])
+    stores = [store_mixed, pltpu.make_async_copy(acc, acc_hbm, out_sem.at[1])]
+    stores.append(pltpu.make_async_copy(weights.at[pl.ds(LAST, GSIZE * CAP), :], last_weights_hbm, out_sem.at[2]))
+    for store in stores[1:]:
+        store.start()
+    group_wait(tbuf, r_recv, GROUPS - 1)
     sent = sbuf.at[pl.ds(0, PEERS - 1)]
     pltpu.make_async_copy(sent, sent, d_send).wait()
     pltpu.make_async_copy(sent, sent, r_send).wait()
     w_wait(w_send.at[0], 6)
     w_wait(w_send.at[1], 18)
     w_wait(w_send.at[2], 24)
-    store_mixed.wait()
-    store_moe.wait()
-
-
-def copy_out(mixed_in, moe_in, mixed_out, moe_out, mixed, moe, sem_in, sem_out):
-    pieces = []
-    for n in range(4):
-        at = pl.ds(n * 256, 256)
-        pieces.append((mixed_in.at[at, :], mixed.at[at, :], mixed_out.at[at, :]))
-    pieces.append((moe_in, moe, moe_out))
-    reads = [pltpu.make_async_copy(a, b, sem_in.at[n]) for n, (a, b, _) in enumerate(pieces)]
-    writes = [pltpu.make_async_copy(b, o, sem_out.at[n]) for n, (_, b, o) in enumerate(pieces)]
-    for read in reads:
+    for store in stores:
+        store.wait()
+
+
+def finish(
+    mixed_in, acc_in, weights_in, last_in, mixed_out, moe_out, mixed, acc, weights, last, scr, rows, moe, sem_in, sem_out
+):
+    firsts = ((last_in, last), (weights_in, weights), (acc_in, acc))
+    firsts = [pltpu.make_async_copy(a, b, sem_in.at[4 + n]) for n, (a, b) in enumerate(firsts)]
+    cuts = [pl.ds(n * 256, 256) for n in range(4)]
+    reads = [pltpu.make_async_copy(mixed_in.at[at, :], mixed.at[at, :], sem_in.at[n]) for n, at in enumerate(cuts)]
+    writes = [pltpu.make_async_copy(mixed.at[at, :], mixed_out.at[at, :], sem_out.at[n]) for n, at in enumerate(cuts)]
+    for read in (firsts[0], *reads[:2], *firsts[1:], *reads[2:]):
         read.start()
-    for read, write in zip(reads, writes):
+    firsts[0].wait()
+
+    for read, write in zip(reads[:2], writes[:2]):
         read.wait()
         write.start()
-    for write in writes:
+
+    def unpack(i, carry):
+        scr[pl.ds(pl.multiple_of(i * PITCH, 8), BLOCK), :] = last[i].astype(F32)
+        return carry
+
+    lax.fori_loop(0, GSIZE, unpack, 0, unroll=4)
+
+    def line_up(n, carry):
+        cols = pl.ds(pl.multiple_of(n * 128, 128), 128)
+        for r in range(CAP):
+            rows[pl.ds(r * GSIZE, GSIZE), cols] = scr[pl.ds(r * PIECES + n, GSIZE, stride=PITCH), :].astype(BF16)
+        return carry
+
+    lax.fori_loop(0, PIECES, line_up, 0)
+    for read, write in zip(reads[2:], writes[2:]):
+        read.wait()
+        write.start()
+    for first in firsts[1:]:
+        first.wait()
+    for n in range(4):
+        cols = pl.ds(n * 512, 512)
+        moe[:, cols] = (acc[:, cols] + weighted(weights[...], rows[:, cols])).astype(BF16)
+    store_moe = pltpu.make_async_copy(moe, moe_out, sem_out.at[4])
+    store_moe.start()
+    for write in (*writes, store_moe):
         write.wait()
 
 
@@ -465,14 +496,16 @@
 ):
     hbm = pl.BlockSpec(memory_space=pl.ANY)
     dma = pltpu.SemaphoreType.DMA
-    mixed, moe_output = pl.pallas_call(
+    made = pl.pallas_call(
         kernel,
         out_shape=(
             jax.ShapeDtypeStruct((1024, 2048), BF16),
-            jax.ShapeDtypeStruct((128, 2048), BF16),
+            jax.ShapeDtypeStruct((128, 2048), F32),
+            jax.ShapeDtypeStruct((GSIZE * CAP, 128), BF16),
+            jax.ShapeDtypeStruct((GSIZE, BLOCK, 128), BF16),
         ),
         in_specs=[hbm] * 14,
-        out_specs=(hbm, hbm),
+        out_specs=(hbm,) * 4,
         scratch_shapes=[
             pltpu.VMEM((31, 1024), F32),
             pltpu.VMEM((1, 1024), F32),
@@ -497,7 +530,7 @@
             pltpu.VMEM((PEERS, BLOCK, 128), BF16),
             pltpu.VMEM((PEERS, BLOCK, 128), BF16),
             pltpu.VMEM((PEERS, BLOCK, 128), BF16),
-            pltpu.VMEM((PEERS, BLOCK, 128), BF16),
+            pltpu.VMEM((PEERS - GSIZE, BLOCK, 128), BF16),
             pltpu.VMEM((GSIZE * PITCH, 128), F32),
             pltpu.VMEM((GSIZE * CAP, 2048), BF16),
             pltpu.VMEM((GSIZE * CAP, 1024), BF16),
@@ -507,8 +540,7 @@
             pltpu.VMEM((PEERS * CAP, 2048), BF16),
             pltpu.VMEM((CAP * PEERS, 128), BF16),
             pltpu.VMEM((128, 2048), F32),
-            pltpu.VMEM((128, 2048), BF16),
-            dma((24,)), dma((2,)),  dma((2,)), dma((2,)), dma((3,)), dma((3,)), dma, dma,
+            dma((24,)), dma((3,)), dma((2,)), dma((2,)), dma((3,)), dma((3,)), dma, dma,
             dma, dma((GROUPS,)), dma, dma((GROUPS,)), dma((2,)),
         ],
         compiler_params=pltpu.CompilerParams(
@@ -520,16 +552,21 @@
         moe_input, moe_gain.reshape(1, -1), expert_ids.T, expert_share.T, places(),
         expert_gate_weight, expert_up_weight, expert_down_weight,
     )
-    shapes = (mixed.shape, moe_output.shape)
     return pl.pallas_call(
-        copy_out,
-        out_shape=tuple(jax.ShapeDtypeStruct(shape, BF16) for shape in shapes),
-        in_specs=[hbm, hbm],
+        finish,
+        out_shape=(jax.ShapeDtypeStruct((1024, 2048), BF16), jax.ShapeDtypeStruct((128, 2048), BF16)),
+        in_specs=[hbm] * 4,
         out_specs=(hbm, hbm),
-        scratch_shapes=[*(pltpu.VMEM(shape, BF16) for shape in shapes), dma((5,)), dma((5,))],
+        scratch_shapes=[
+            *(pltpu.VMEM(array.shape, array.dtype) for array in made),
+            pltpu.VMEM((GSIZE * PITCH, 128), F32),
+            pltpu.VMEM((GSIZE * CAP, 2048), BF16),
+            pltpu.VMEM((128, 2048), BF16),
+            dma((7,)), dma((5,)),
+        ],
         compiler_params=pltpu.CompilerParams(vmem_limit_bytes=63 * 2**20),
-        name="copy_out",
-    )(mixed, moe_output)
+        name="finish",
+    )(*made)
 
 
 def solution(mesh):

time: 92.6 us -> 93.3 us (level)
    pallas_call x1, Pallas kernels: 88.2 us -> 86.9 us  [body(): pl.pallas_call(kernel, out_shape=(jax.ShapeDtypeStruct((1024, 2048), BF16...]
    pallas_call x1, Pallas kernels: 3.63 us -> 4.79 us  [body(): pl.pallas_call(finish, out_shape=(jax.ShapeDtypeStruct((1024, 2048), BF16...]
where the time goes in v5:
time: 93.3 us; the launch traced here: 92.3 us
  Pallas kernels  91.7 us (98%)
    pallas_call x1, Pallas kernels, body(): pl.pallas_call(kernel, out_shape=(jax.ShapeDtypeStruct((1024, 2048), BF16...  86.9 us
    pallas_call x1, Pallas kernels, body(): pl.pallas_call(finish, out_shape=(jax.ShapeDtypeStruct((1024, 2048), BF16...  4.79 us

profile of v5, /device:TPU:1, one launch (start us, length us, event | category | flops | bytes accessed | tf_op | source)
XLA Modules:
  0.0 92.3 jit_solution(4958773993361335988)
XLA Ops:
  0.6 86.9 %mixer.1 = (bf16[1024,2048]{1,0:T(8,128)(2,1)}, f32[128,2048]{1,0:T(8,128)}, bf16[160,128]{1,0:T(8,128)(2,1)}, bf16[32,80,128]{2,1,0:T(8,128)(2,1)}) custom-call(bf16[1024,1024]{1,0:T(8,128)(2,1)} %value_hbm.1, bf16[1024,1024]{1,0:T(8,128)(2,1)} %gate_hbm.1, f32[31,1024]{1,0:T(8,128)} %taps_hbm.1, f32[1,1024]{1,0:T(1,128)} %bitcast.6, f32[1,1024]{1,0:T(1,128)} %bitcast.7, ...), custom_call_target="tpu_custom_call" | custom-call | tf_op jit(solution)/shard_map/mixer/pallas_call | solution.py:499
  87.5 4.8 %finish.1 = (bf16[1024,2048]{1,0:T(8,128)(2,1)}, bf16[128,2048]{1,0:T(8,128)(2,1)}) custom-call(bf16[1024,2048]{1,0:T(8,128)(2,1)} %get-tuple-element.6.mixed_in, f32[128,2048]{1,0:T(8,128)} %get-tuple-element.7.acc_in, bf16[160,128]{1,0:T(8,128)(2,1)} %get-tuple-element.8.weights_in, bf16[32,80,128]{2,1,0:T(8,128)(2,1)} %get-tuple-element.9.last_in), custom_call_target="tpu_custom_call" | custom-call | tf_op jit(solution)/shard_map/finish/pallas_call | solution.py:555
